TPU v7x, 128 devices: a whole 4x4x4 slice. The times are simulated.
128 devices in a mesh: ep: 64 (over z, y, x), tp: 2 (over core).
Axes of the slice: x: 4, y: 4, z: 4, core: 2. Of those that a mesh axis runs over, the one named last changes fastest.
Arguments:
- hidden: bfloat16 [1408, 2048], P('ep'), may hold values from -6 to 6
- mixer_gain: bfloat16 [2048], replicated, may hold values from 0.099609375 to 1.8984375
- gate_proj: bfloat16 [2048, 1024], P(None, 'tp'), may hold values from -0.125 to 0.125
- value_proj: bfloat16 [2048, 1024], P(None, 'tp'), may hold values from -0.125 to 0.125
- write_proj: bfloat16 [2048, 512], P(None, 'tp'), may hold values from -0.125 to 0.125
- read_proj: bfloat16 [2048, 512], P(None, 'tp'), may hold values from -0.125 to 0.125
- step_proj: bfloat16 [2048, 16], replicated, may hold values from -0.125 to 0.125
- step_bias: float32 [16], replicated, may hold values from -3 to 0
- decay_log: float32 [16], replicated, may hold values from 0 to 2.77
- skip_gain: float32 [16], replicated, may hold values from 0.5 to 2
- value_taps: bfloat16 [4, 1024], replicated, may hold values from -3 to 3
- write_taps: bfloat16 [4, 512], replicated, may hold values from -3 to 3
- read_taps: bfloat16 [4, 512], replicated, may hold values from -3 to 3
- value_tail: bfloat16 [1408, 3, 1024], P('ep', None, 'tp'), may hold values from -6 to 6
- write_tail: bfloat16 [1408, 3, 512], P('ep', None, 'tp'), may hold values from -6 to 6
- read_tail: bfloat16 [1408, 3, 512], P('ep', None, 'tp'), may hold values from -6 to 6
- scan_state: float32 [1408, 16, 64, 128], P('ep', 'tp'), may hold values from -4 to 4
- group_gain: bfloat16 [1024], replicated, may hold values from 0.099609375 to 1.8984375
- out_proj: bfloat16 [1024, 2048], P('tp'), may hold values from -0.1875 to 0.1875
- ffn_gain: bfloat16 [2048], replicated, may hold values from 0.099609375 to 1.8984375
- group_router: bfloat16 [2048, 8], replicated, may hold values from -0.125 to 0.125
- expert_router: bfloat16 [2048, 64], replicated, may hold values from -0.125 to 0.125
- expert_choice: int32 [1408, 3], P('ep'), may hold values from 0 to 63, as said below
- expert_gate: bfloat16 [64, 2048, 1024], P('ep', None, 'tp'), may hold values from -0.125 to 0.125
- expert_up: bfloat16 [64, 2048, 1024], P('ep', None, 'tp'), may hold values from -0.125 to 0.125
- expert_down: bfloat16 [64, 1024, 2048], P('ep', 'tp'), may hold values from -1 to 1
Outputs:
- layer_out: bfloat16 [1408, 2048], P('ep', 'tp')
- new_state: float32 [1408, 16, 64, 128], P('ep', 'tp')
Inputs may be any that keep to these rules, and one draw needn't show every extreme that they name: `expert_choice`: every row names 3 different experts of one group (numbers equal in // 8). The 22 rows of one device name no expert more than 3 times, and for every device some expert is named exactly 3 times.
All inputs are finite; a program needn't handle non-finite values.
Results may differ from a plain program's by a relative error of at most 0.017.
Values may be sent and summed in bfloat16 or wider, within the bound.
A program may use at most 128 MiB of HBM per device.

v0:
```python
import jax
import jax.numpy as jnp
from jax import lax
from jax.sharding import PartitionSpec as P

GROUP_SIZE = 8


EPSILON = 1e-06


def sent_to_all(array, axis):
    peers = lax.axis_size(axis)
    return lax.all_to_all(
        jnp.broadcast_to(array[None], (peers, *array.shape)), axis, 0, 0, tiled=True
    )


def of_everyone(array, axis):
    return sent_to_all(array, axis).sum(axis=0)


def cut_along(array, dim, peers):
    dims = array.shape
    tiles = array.reshape(*dims[:dim], peers, dims[dim] // peers, *dims[dim + 1 :])
    return jnp.moveaxis(tiles, dim, 0)


def sum_at_owner(array, axis, dim):
    peers = lax.axis_size(axis)
    tiles = lax.all_to_all(cut_along(array, dim, peers), axis, 0, 0, tiled=True)
    return jnp.sum(tiles.astype(jnp.float32), axis=0)


def in_order(tiles, dim):
    dims = list(tiles.shape[1:])
    dims[dim] *= tiles.shape[0]
    return jnp.moveaxis(tiles, 0, dim).reshape(dims)


def gathered_copies(array, axis, dim):
    tiles = sent_to_all(array, axis)
    return in_order(tiles, dim)


def normed(values, gain):
    widened = values.astype(jnp.float32)
    scale = lax.rsqrt(jnp.mean(widened * widened, axis=-1, keepdims=True) + EPSILON)
    return widened * scale * gain.astype(jnp.float32)


def convolve(history, newest, kernel):
    summed = kernel[-1].astype(jnp.float32) * newest.astype(jnp.float32)
    for offset in range(history.shape[1]):
        summed = summed + kernel[offset].astype(jnp.float32) * history[:, offset].astype(
            jnp.float32
        )
    return jax.nn.silu(summed)


def project(left, right):
    return jnp.dot(left, right, preferred_element_type=jnp.float32)


def on_device(
    hidden,
    mixer_gain,
    gate_proj,
    value_proj,
    write_proj,
    read_proj,
    step_proj,
    step_bias,
    decay_log,
    skip_gain,
    value_taps,
    write_taps,
    read_taps,
    value_tail,
    write_tail,
    read_tail,
    scan_state,
    group_gain,
    out_proj,
    ffn_gain,
    group_router,
    expert_router,
    expert_choice,
    expert_gate,
    expert_up,
    expert_down,
):
    tp_count = lax.axis_size("tp")
    ep_count = lax.axis_size("ep")
    tp_index = lax.axis_index("tp")
    seq_rows = hidden.shape[0]
    mixer_in = normed(hidden, mixer_gain).astype(jnp.bfloat16)
    gate_new = project(mixer_in, gate_proj).astype(jnp.bfloat16)
    value_new = project(mixer_in, value_proj).astype(jnp.bfloat16)
    write_new = project(mixer_in, write_proj).astype(jnp.bfloat16)
    read_new = project(mixer_in, read_proj).astype(jnp.bfloat16)
    head_count = step_proj.shape[1] // tp_count
    head_start = tp_index * head_count
    step_local = lax.dynamic_slice_in_dim(step_proj, head_start, head_count, 1)
    bias_local = lax.dynamic_slice_in_dim(step_bias, head_start, head_count, 0)
    rate_local = jnp.exp(lax.dynamic_slice_in_dim(decay_log, head_start, head_count, 0))
    skip_local = lax.dynamic_slice_in_dim(skip_gain, head_start, head_count, 0)
    step_size = jax.nn.softplus(project(mixer_in, step_local) + bias_local)
    decay = jnp.exp(-step_size * rate_local)
    value_width = value_proj.shape[1]
    vector_width = write_proj.shape[1]
    value_conv = convolve(
        value_tail,
        value_new,
        lax.dynamic_slice_in_dim(value_taps, tp_index * value_width, value_width, 1),
    )
    write_conv = convolve(
        write_tail,
        write_new,
        lax.dynamic_slice_in_dim(write_taps, tp_index * vector_width, vector_width, 1),
    )
    read_conv = convolve(
        read_tail,
        read_new,
        lax.dynamic_slice_in_dim(read_taps, tp_index * vector_width, vector_width, 1),
    )
    state_size = scan_state.shape[3]
    group_count = vector_width // state_size
    per_group = head_count // group_count
    heads_value = value_conv.reshape(seq_rows, head_count, value_width // head_count)
    heads_write = jnp.repeat(
        write_conv.reshape(seq_rows, group_count, state_size), per_group, axis=1
    )
    heads_read = jnp.repeat(read_conv.reshape(seq_rows, group_count, state_size), per_group, axis=1)
    new_state = (
        decay[:, :, None, None] * scan_state
        + (step_size[:, :, None] * heads_value)[:, :, :, None] * heads_write[:, :, None, :]
    )
    mixed_heads = (
        jnp.einsum("thpn,thn->thp", new_state, heads_read) + skip_local[None, :, None] * heads_value
    )
    gated = mixed_heads.reshape(seq_rows, value_width) * jax.nn.silu(gate_new.astype(jnp.float32))
    grouped = gated.reshape(seq_rows, group_count, value_width // group_count)
    grouped = grouped * lax.rsqrt(jnp.mean(grouped * grouped, axis=-1, keepdims=True) + EPSILON)
    gain_local = lax.dynamic_slice_in_dim(group_gain, tp_index * value_width, value_width, 0)
    mixed = (grouped.reshape(seq_rows, value_width) * gain_local.astype(jnp.float32)).astype(
        jnp.bfloat16
    )
    residual = hidden.astype(jnp.float32) + of_everyone(project(mixed, out_proj), "tp")
    ffn_in = normed(residual, ffn_gain).astype(jnp.bfloat16)
    group_weights = jnp.exp(project(ffn_in, group_router))
    group_prob = group_weights / jnp.sum(group_weights, axis=1, keepdims=True)
    group_of = expert_choice[:, 0] // GROUP_SIZE
    group_mask = jnp.arange(group_router.shape[1])[None, :] == group_of[:, None]
    chosen_prob = jnp.sum(jnp.where(group_mask, group_prob, 0.0), axis=1, keepdims=True)
    picked_exp = jnp.exp(jnp.take_along_axis(project(ffn_in, expert_router), expert_choice, axis=1))
    gates = chosen_prob * picked_exp / jnp.sum(picked_exp, axis=1, keepdims=True)
    experts_total = expert_router.shape[1]
    top_count = expert_choice.shape[1]
    capacity = top_count * ((seq_rows + experts_total - 1) // experts_total)
    flat_choice = expert_choice.reshape(-1)
    one_hot = (flat_choice[:, None] == jnp.arange(experts_total)[None, :]).astype(jnp.int32)
    earlier = jnp.cumsum(one_hot, axis=0) - one_hot
    position = jnp.sum(earlier * one_hot, axis=1)
    target = (flat_choice * capacity + position).reshape(seq_rows, top_count)
    routing = target[:, :, None] == jnp.arange(experts_total * capacity)[None, None, :]
    dispatch = jnp.any(routing, axis=1).T.astype(jnp.bfloat16)
    combine = jnp.sum(routing.astype(jnp.float32) * gates[:, :, None], axis=1)
    model_width = ffn_in.shape[1]
    half_width = model_width // tp_count
    own_columns = lax.dynamic_slice_in_dim(ffn_in, tp_index * half_width, half_width, 1)
    outgoing = (
        project(dispatch, own_columns).astype(jnp.bfloat16).reshape(ep_count, capacity, half_width)
    )
    arrived = gathered_copies(
        lax.all_to_all(outgoing, "ep", split_axis=0, concat_axis=0, tiled=True), "tp", 2
    )
    slot_total = arrived.shape[1]
    flat_rows = arrived.reshape(-1, model_width)
    activated = (
        jax.nn.silu(project(flat_rows, expert_gate[0])) * project(flat_rows, expert_up[0])
    ).astype(jnp.bfloat16)
    partial_value = project(activated, expert_down[0]).reshape(ep_count, slot_total, model_width)
    reduced = sum_at_owner(partial_value.astype(jnp.bfloat16), "tp", 2).astype(jnp.bfloat16)
    returned = lax.all_to_all(reduced, "ep", split_axis=0, concat_axis=0, tiled=True)
    expert_sum = jnp.dot(combine, returned.reshape(-1, half_width).astype(jnp.float32))
    residual_half = lax.dynamic_slice_in_dim(residual, tp_index * half_width, half_width, 1)
    layer_out = (residual_half + expert_sum).astype(jnp.bfloat16)
    return (layer_out, new_state)


def solution(mesh):
    placed = (
        P("ep", None),
        P(),
        P(None, "tp"),
        P(None, "tp"),
        P(None, "tp"),
        P(None, "tp"),
        P(),
        P(),
        P(),
        P(),
        P(),
        P(),
        P(),
        P("ep", None, "tp"),
        P("ep", None, "tp"),
        P("ep", None, "tp"),
        P("ep", "tp", None, None),
        P(),
        P("tp", None),
        P(),
        P(),
        P(),
        P("ep", None),
        P("ep", None, "tp"),
        P("ep", None, "tp"),
        P("ep", "tp", None),
    )
    return jax.shard_map(
        on_device,
        mesh=mesh,
        in_specs=placed,
        out_specs=(P("ep", "tp"), P("ep", "tp", None, None)),
        check_vma=False,
    )
```

profile of v0, /device:TPU:1, one launch (start us, length us, event | category | flops | bytes accessed | tf_op | source)
XLA Modules:
  0.0 92.0 jit_solution(779154019292126479)
XLA Ops:
  0.7 0.9 dynamic_slice.31
  3.0 1.0 %fusion.28 = f32[22]{0:T(128)S(1)} fusion(bf16[22,2048]{1,0:T(8,128)(2,1)} %param.26), kind=kLoop, calls=%fused_computation.39 | loop fusion | flops 135146 | bytes 90200 | tf_op jit(solution)/shard_map/reduce_sum | solution.py:48
  4.8 1.1 %multiply_exponential_fusion = (f32[22,8]{0,1:T(8,128)S(1)}, f32[22,8]{0,1:T(8,128)S(1)}) fusion(f32[8]{0:T(128)S(1)} %dynamic-slice_exponential_fusion, f32[8]{0:T(128)S(1)} %dynamic_slice.31, bf16[2048,16]{0,1:T(8,128)(2,1)} %param.32, s32[]{:T(128)S(6)} %select_n.42, bf16[22,2048]{1,0:T(8,128)(2,1)} %param.26, f32[2048]{0:T(1024)S(1)} %convert_element_type.145, ...), kind=kOutput, calls=%fused_computation.76 | convolution fusion | flops 902704 | bytes 140828 | tf_op jit(solution)/shard_map/dot_general | solution.py:62
  6.8 0.9 dynamic-slice_convert_fusion.3
  7.8 0.9 dynamic-slice_convert_fusion.6
  8.7 1.5 %divide_multiply_fusion.2 = f32[22,256]{1,0:T(8,128)S(1)} fusion(bf16[2048,256]{1,0:T(8,128)(2,1)} %param.30, bf16[22,3,256]{2,0,1:T(8,128)(2,1)} %param.40, f32[256]{0:T(256)S(1)} %bitcast.116, f32[256]{0:T(256)S(1)} %bitcast.118, f32[256]{0:T(256)S(1)} %bitcast.117, f32[256]{0:T(256)S(1)} %bitcast.119, bf16[22,2048]{1,0:T(8,128)(2,1)} %param.26, ...), kind=kOutput, calls=%fused_computation.70 | convolution fusion | flops 23339008 | bytes 1207384 | tf_op jit(solution)/shard_map/dot_general | solution.py:62
  10.2 1.5 %divide_multiply_fusion.1 = f32[22,256]{1,0:T(8,128)S(1)} fusion(bf16[2048,256]{1,0:T(8,128)(2,1)} %param.31, bf16[22,3,256]{2,0,1:T(8,128)(2,1)} %param.41, f32[256]{0:T(256)S(1)} %bitcast.115, f32[256]{0:T(256)S(1)} %bitcast.113, f32[256]{0:T(256)S(1)} %bitcast.114, f32[256]{0:T(256)S(1)} %bitcast.112, bf16[22,2048]{1,0:T(8,128)(2,1)} %param.26, ...), kind=kOutput, calls=%fused_computation.69 | convolution fusion | flops 23339008 | bytes 1207384 | tf_op jit(solution)/shard_map/dot_general | solution.py:62
  11.8 2.1 %divide_multiply_fusion = f32[22,512]{1,0:T(8,128)S(1)} fusion(bf16[2048,512]{1,0:T(8,128)(2,1)} %param.29, bf16[22,3,512]{2,0,1:T(8,128)(2,1)} %param.39, f32[512]{0:T(512)S(1)} %bitcast.111, f32[512]{0:T(512)S(1)} %bitcast.109, f32[512]{0:T(512)S(1)} %bitcast.110, f32[512]{0:T(512)S(1)} %bitcast.108, bf16[22,2048]{1,0:T(8,128)(2,1)S(1)} %copy-done.2, ...), kind=kOutput, calls=%fused_computation.55 | convolution fusion | flops 46497792 | bytes 2316376 | tf_op jit(solution)/shard_map/dot_general | solution.py:62
  14.1 4.6 %multiply_add_fusion = f32[22,8,64,128]{3,2,1,0:T(8,128)S(1)} fusion(f32[22,8,64,128]{3,2,1,0:T(8,128)} %param.42, f32[22,8,128]{2,1,0:T(8,128)S(1)} %bitcast.103, f32[22,8,64]{2,1,0:T(8,128)S(1)} %broadcast_multiply_fusion, f32[22,8]{1,0:T(8,128)S(1)} %copy.130), kind=kLoop, calls=%fused_computation.1 | loop fusion | flops 4325376 | bytes 11670208 | tf_op jit(solution)/shard_map/add | solution.py:136
  18.7 1.6 %fusion.53 = f32[22,8,1,64]{3,2,1,0:T(1,128)S(1)} fusion(f32[22,8,64,128]{3,2,1,0:T(8,128)S(1)} %multiply_add_fusion, f32[22,8,128,1]{2,3,1,0:T(1,128)S(1)} %bitcast.105), kind=kOutput, calls=%fused_computation.109 | convolution fusion | flops 2883584 | bytes 5902336 | tf_op jit(solution)/shard_map/thpn,thn->thp/dot_general | solution.py:140
  20.3 0.9 copy-done.1
  21.4 2.0 %fusion.51 = (f32[22,512]{1,0:T(8,128)S(1)}, f32[22,512]{1,0:T(8,128)S(1)}) fusion(f32[22,512]{1,0:T(8,128)S(1)} %reshape.134, bf16[2048,512]{1,0:T(8,128)(2,1)} %param.28, bf16[22,2048]{1,0:T(8,128)(2,1)S(1)} %copy-done.2, f32[2048]{0:T(1024)S(1)} %convert_element_type.145, f32[22]{0:T(128)S(1)} %add_rsqrt_fusion.2), kind=kOutput, calls=%fused_computation.107 | convolution fusion | flops 46407680 | bytes 2330712 | tf_op jit(solution)/shard_map/dot_general | solution.py:62
  23.7 2.0 %fusion.36 = f32[22,2048]{1,0:T(8,128)S(1)} fusion(bf16[512,2048]{1,0:T(8,128)(2,1)} %param.44, f32[22,512]{1,0:T(8,128)S(1)} %get-tuple-element.19, f32[22,512]{1,0:T(8,128)S(1)} %bitcast.107, f32[512]{0:T(512)S(1)} %dynamic-slice_convert_fusion.10), kind=kOutput, calls=%fused_computation.61 | convolution fusion | flops 46171136 | bytes 2369536 | tf_op jit(solution)/shard_map/dot_general | solution.py:62
  26.5 4.8 %all-to-all-start = ((f32[2,22,2048]{2,1,0:T(8,128)}), f32[2,22,2048]{2,1,0:T(8,128)S(1)}, u32[]{:S(2)}, u32[]{:S(2)}) async-start(f32[2,22,2048]{2,1,0:T(8,128)} %broadcast_in_dim.14), calls=%async_computation | async-start | bytes 786432 | tf_op jit(solution)/shard_map/all_to_all | solution.py:14
  33.2 1.0 %reshape.136 = bf16[64,3,1024]{2,1,0:T(4,128)(2,1)} reshape(bf16[192,1024]{1,0:T(8,128)(2,1)S(1)} %convolution_convert_fusion.1) | data formatting | bytes 786432 | tf_op jit(solution)/shard_map/reshape | solution.py:173
  34.2 11.2 %all-to-all-start.1 = ((bf16[64,3,1024]{2,1,0:T(4,128)(2,1)}), bf16[64,3,1024]{2,1,0:T(4,128)(2,1)S(1)}, u32[]{:S(2)}, u32[]{:S(2)}) async-start(bf16[64,3,1024]{2,1,0:T(4,128)(2,1)} %reshape.136), calls=%async_computation.1 | async-start | bytes 1048576 | tf_op jit(solution)/shard_map/all_to_all | solution.py:176
  45.9 1.7 %gather_fusion = f32[66]{0:T(128)S(1)} fusion(f32[22,64]{1,0:T(8,128)S(1)} %fusion.54, s32[66]{0:T(128)S(1)} %reshape.160), kind=kCustom, calls=%fused_computation | custom fusion | bytes 1056 | tf_op jit(solution)/shard_map/jit(take_along_axis)/gather | solution.py:156
  48.0 9.9 %all-to-all-done.1 = bf16[64,3,1024]{2,1,0:T(4,128)(2,1)S(1)} async-done(((bf16[64,3,1024]{2,1,0:T(4,128)(2,1)}), bf16[64,3,1024]{2,1,0:T(4,128)(2,1)S(1)}, u32[]{:S(2)}, u32[]{:S(2)}) %all-to-all-start.1) | async-done | bytes 393248 | tf_op jit(solution)/shard_map/all_to_all | solution.py:176
  58.2 6.0 %all_to_all.25 = bf16[2,64,3,1024]{3,1,2,0:T(8,128)(2,1)S(1)} all-to-all(bf16[2,64,3,1024]{3,1,2,0:T(8,128)(2,1)S(1)} %broadcast_in_dim.16), channel_id=1, replica_groups=mesh['ep'=64,'tp'=2] {'tp'}, dimensions={0} | all-to-all | bytes 1572864 | tf_op jit(solution)/shard_map/all_to_all | solution.py:14
  64.2 0.8 copy.138
  68.0 4.4 %all_to_all.26 = bf16[2,64,3,1024]{3,1,2,0:T(8,128)(2,1)S(1)} all-to-all(bf16[2,64,3,1024]{3,1,2,0:T(8,128)(2,1)S(1)} %bitcast.99), channel_id=1, replica_groups=mesh['ep'=64,'tp'=2] {'tp'}, dimensions={0} | all-to-all | bytes 1572864 | tf_op jit(solution)/shard_map/all_to_all | solution.py:31
  72.5 1.1 %copy.142 = bf16[64,3,1024]{2,1,0:T(4,128)(2,1)} copy(bf16[64,3,1024]{2,0,1:T(8,128)(2,1)S(1)} %reduce_sum.105) | data formatting | bytes 786432 | tf_op jit(solution)/shard_map/reduce_sum | solution.py:32
  73.6 4.6 %all-to-all-start.4 = ((bf16[64,3,1024]{2,1,0:T(4,128)(2,1)}), bf16[64,3,1024]{2,1,0:T(4,128)(2,1)S(1)}, u32[]{:S(2)}, u32[]{:S(2)}) async-start(bf16[64,3,1024]{2,1,0:T(4,128)(2,1)} %copy.142), calls=%async_computation.4 | async-start | bytes 1048576 | tf_op jit(solution)/shard_map/all_to_all | solution.py:185
  78.4 12.5 %all-to-all-done.4 = bf16[64,3,1024]{2,1,0:T(4,128)(2,1)S(1)} async-done(((bf16[64,3,1024]{2,1,0:T(4,128)(2,1)}), bf16[64,3,1024]{2,1,0:T(4,128)(2,1)S(1)}, u32[]{:S(2)}, u32[]{:S(2)}) %all-to-all-start.4) | async-done | bytes 393248 | tf_op jit(solution)/shard_map/all_to_all | solution.py:185
  (78 shorter events, 11.7 us)
Async XLA Ops:
  0.6 66.7 %copy-start = (bf16[1,512,2048]{2,1,0:T(8,128)(2,1)S(1)}, bf16[1,512,2048]{2,1,0:T(8,128)(2,1)}, u32[]{:S(2)}) copy-start(bf16[1,512,2048]{2,1,0:T(8,128)(2,1)} %param.51) | copy-start | bytes 6291460
  0.6 11.2 %copy-start.2 = (bf16[22,2048]{1,0:T(8,128)(2,1)S(1)}, bf16[22,2048]{1,0:T(8,128)(2,1)}, u32[]{:S(2)}) copy-start(bf16[22,2048]{1,0:T(8,128)(2,1)} %param.26) | copy-start | bytes 270340
  18.7 2.5 %copy-start.1 = (f32[22,8,64,128]{3,2,1,0:T(8,128)}, f32[22,8,64,128]{3,2,1,0:T(8,128)S(1)}, u32[]{:S(2)}) copy-start(f32[22,8,64,128]{3,2,1,0:T(8,128)S(1)} %multiply_add_fusion) | copy-start | bytes 17301508
  23.4 7.9 %copy-start.7 = (bf16[2048]{0:T(1024)(128)(2,1)S(1)}, bf16[2048]{0:T(1024)(128)(2,1)}, u32[]{:S(2)}) copy-start(bf16[2048]{0:T(1024)(128)(2,1)} %param.45) | copy-start | bytes 12292
  23.4 7.9 %copy-start.5 = (s32[22,3]{0,1:T(4,128)S(1)}, s32[22,3]{0,1:T(4,128)}, u32[]{:S(2)}) copy-start(s32[22,3]{0,1:T(4,128)} %param.48) | copy-start | bytes 796
  26.5 6.1 %all-to-all-start = ((f32[2,22,2048]{2,1,0:T(8,128)}), f32[2,22,2048]{2,1,0:T(8,128)S(1)}, u32[]{:S(2)}, u32[]{:S(2)}) async-start(f32[2,22,2048]{2,1,0:T(8,128)} %broadcast_in_dim.14), calls=%async_computation | async-start | bytes 786432 | tf_op jit(solution)/shard_map/all_to_all | solution.py:14
  31.3 14.2 %copy-start.4 = (bf16[2048,64]{0,1:T(8,128)(2,1)S(1)}, bf16[2048,64]{0,1:T(8,128)(2,1)}, u32[]{:S(2)}) copy-start(bf16[2048,64]{0,1:T(8,128)(2,1)} %param.47) | copy-start | bytes 786436
  34.2 23.7 %all-to-all-start.1 = ((bf16[64,3,1024]{2,1,0:T(4,128)(2,1)}), bf16[64,3,1024]{2,1,0:T(4,128)(2,1)S(1)}, u32[]{:S(2)}, u32[]{:S(2)}) async-start(bf16[64,3,1024]{2,1,0:T(4,128)(2,1)} %reshape.136), calls=%async_computation.1 | async-start | bytes 1048576 | tf_op jit(solution)/shard_map/all_to_all | solution.py:176
  45.9 1.9 %copy-start.6 = (bf16[2048,8]{0,1:T(8,128)(2,1)S(1)}, bf16[2048,8]{0,1:T(8,128)(2,1)}, u32[]{:S(2)}) copy-start(bf16[2048,8]{0,1:T(8,128)(2,1)} %param.46) | copy-start | bytes 98308
  58.2 7.0 %copy-start.3 = (bf16[1,2048,512]{2,1,0:T(8,128)(2,1)S(1)}, bf16[1,2048,512]{2,1,0:T(8,128)(2,1)}, u32[]{:S(2)}) copy-start(bf16[1,2048,512]{2,1,0:T(8,128)(2,1)} %param.49) | copy-start | bytes 6291460
  65.0 1.6 %copy-start.8 = (bf16[1,2048,512]{2,1,0:T(8,128)(2,1)S(1)}, bf16[1,2048,512]{2,1,0:T(8,128)(2,1)}, u32[]{:S(2)}) copy-start(bf16[1,2048,512]{2,1,0:T(8,128)(2,1)} %param.50) | copy-start | bytes 6291460
  73.6 17.3 %all-to-all-start.4 = ((bf16[64,3,1024]{2,1,0:T(4,128)(2,1)}), bf16[64,3,1024]{2,1,0:T(4,128)(2,1)S(1)}, u32[]{:S(2)}, u32[]{:S(2)}) async-start(bf16[64,3,1024]{2,1,0:T(4,128)(2,1)} %copy.142), calls=%async_computation.4 | async-start | bytes 1048576 | tf_op jit(solution)/shard_map/all_to_all | solution.py:185
where the time goes:
time: 93.2 us; the launch traced here: 92 us
  waiting for transfers between devices  22.8 us (24%)
  starting transfers between devices  20.7 us (22%)
  matrix products  15.1 us (16%)
  local copies, waits for them, and re-layouts  11.7 us (13%)
  blocking collectives  10.4 us (11%)
  other arithmetic  10.2 us (11%)
  between operations  1.06 us (1%)
    dot_general x12, matrix products, project(): return jnp.dot(left, right, preferred_element_type=jnp.float32)  12.7 us
    all_to_all x1, waiting for transfers between devices, on_device(): lax.all_to_all(reduced, 'ep', split_axis=0, concat_axis=0, tiled=True)  12.5 us
    all_to_all x1, starting transfers between devices, on_device(): lax.all_to_all(outgoing, 'ep', split_axis=0, concat_axis=0, tiled=True)  11.2 us
    all_to_all x1, waiting for transfers between devices, on_device(): lax.all_to_all(outgoing, 'ep', split_axis=0, concat_axis=0, tiled=True)  9.93 us
    all_to_all x1, blocking collectives, sent_to_all(): lax.all_to_all(jnp.broadcast_to(array[None], (peers, *array.shape)), axis...  6.01 us
    all_to_all x1, starting transfers between devices, sent_to_all(): lax.all_to_all(jnp.broadcast_to(array[None], (peers, *array.shape)), axis...  4.84 us
    all_to_all x1, starting transfers between devices, on_device(): lax.all_to_all(reduced, 'ep', split_axis=0, concat_axis=0, tiled=True)  4.63 us
    add x1, other arithmetic, on_device(): decay[:, :, None, None] * scan_state  4.56 us
  transfers between devices with their start and end apart: 3, of which 3 were waited for; matrix products, arithmetic and copies ran while one was open for 4% of the time, Pallas kernels for 0%

commit v1 on v0

--- a/solution.py
+++ b/solution.py
@@ -1,6 +1,8 @@
 import jax
 import jax.numpy as jnp
 from jax import lax
+from jax.experimental import pallas as pl
+from jax.experimental.pallas import tpu as pltpu
 from jax.sharding import PartitionSpec as P
 
 GROUP_SIZE = 8
@@ -9,38 +11,355 @@
 EPSILON = 1e-06
 
 
-def sent_to_all(array, axis):
-    peers = lax.axis_size(axis)
-    return lax.all_to_all(
-        jnp.broadcast_to(array[None], (peers, *array.shape)), axis, 0, 0, tiled=True
-    )
-
-
-def of_everyone(array, axis):
-    return sent_to_all(array, axis).sum(axis=0)
-
-
-def cut_along(array, dim, peers):
-    dims = array.shape
-    tiles = array.reshape(*dims[:dim], peers, dims[dim] // peers, *dims[dim + 1 :])
-    return jnp.moveaxis(tiles, dim, 0)
-
-
-def sum_at_owner(array, axis, dim):
-    peers = lax.axis_size(axis)
-    tiles = lax.all_to_all(cut_along(array, dim, peers), axis, 0, 0, tiled=True)
-    return jnp.sum(tiles.astype(jnp.float32), axis=0)
-
-
-def in_order(tiles, dim):
-    dims = list(tiles.shape[1:])
-    dims[dim] *= tiles.shape[0]
-    return jnp.moveaxis(tiles, 0, dim).reshape(dims)
-
-
-def gathered_copies(array, axis, dim):
-    tiles = sent_to_all(array, axis)
-    return in_order(tiles, dim)
+SIDE = 4
+PEERS = 64
+SLOTS = 3
+WIDTH = 2048
+HALF = 1024
+HIDDEN = 512
+TILES = 8
+ROWS = SLOTS * TILES
+PLANE = 16 * ROWS
+TOTAL = PEERS * ROWS
+SEQ = 22
+PAD = 24
+SPREAD = TILES * PAD
+BF = jnp.bfloat16
+F32 = jnp.float32
+
+
+def nt_dot(left, right):
+    return lax.dot_general(left, right, (((1,), (1,)), ((), ())), preferred_element_type=F32)
+
+
+def project(left, right):
+    return jnp.dot(left, right, preferred_element_type=jnp.float32)
+
+
+def iota(shape, dim):
+    return lax.broadcasted_iota(jnp.int32, shape, dim)
+
+
+def moe_kernel(
+    part_ref,
+    hid_ref,
+    gain_ref,
+    group_ref,
+    expert_ref,
+    choice_ref,
+    gate_hbm,
+    up_hbm,
+    down_hbm,
+    out_ref,
+    wg,
+    wu,
+    wd,
+    part_in,
+    resid,
+    send,
+    recv,
+    recv_sib,
+    comb,
+    perm,
+    perm_back,
+    rows_own,
+    rows_sib,
+    act,
+    y_own,
+    y_out,
+    y_in,
+    back,
+    ret,
+    w_sem,
+    p_send,
+    p_recv,
+    d_send,
+    d_recv,
+    f_send,
+    f_recv,
+    s_send,
+    s_recv,
+    r_send,
+    r_recv,
+):
+    me = lax.axis_index("ep")
+    tp = lax.axis_index("tp")
+    mx, my, mz = me % SIDE, (me // SIDE) % SIDE, me // (SIDE * SIDE)
+
+    def ahead(i):
+        x = (mx + i % SIDE) % SIDE
+        y = (my + (i // SIDE) % SIDE) % SIDE
+        z = (mz + i // (SIDE * SIDE)) % SIDE
+        return (z * SIDE + y) * SIDE + x
+
+    def behind(i):
+        x = (mx + SIDE - i % SIDE) % SIDE
+        y = (my + SIDE - (i // SIDE) % SIDE) % SIDE
+        z = (mz + SIDE - i // (SIDE * SIDE)) % SIDE
+        return (z * SIDE + y) * SIDE + x
+
+    sibling = {"tp": 1 - tp}
+
+    def block(i):
+        return pl.ds(pl.multiple_of(i * ROWS, TILES), ROWS)
+
+    bar = pltpu.get_barrier_semaphore()
+    pl.semaphore_signal(bar, inc=1, device_id=sibling)
+
+    @pl.loop(1, PEERS)
+    def _(i):
+        pl.semaphore_signal(bar, inc=1, device_id={"ep": ahead(i)})
+
+    loads = [
+        pltpu.make_async_copy(gate_hbm, wg, w_sem.at[0]),
+        pltpu.make_async_copy(up_hbm, wu, w_sem.at[1]),
+        pltpu.make_async_copy(down_hbm, wd, w_sem.at[2]),
+    ]
+    for load in loads:
+        load.start()
+
+    diagonal = iota((PAD, SEQ), 0) == iota((PAD, SEQ), 1)
+    earlier = iota((PAD, SEQ), 1) < iota((PAD, SEQ), 0)
+    valid = iota((PAD, 1), 0) < SEQ
+    lines = [choice_ref[k : k + 1, :].astype(F32) for k in range(SLOTS)]
+    chosen = [jnp.sum(jnp.where(diagonal, line, 0.0), axis=1, keepdims=True) for line in lines]
+    codes = []
+    for k in range(SLOTS):
+        same = jnp.zeros((PAD, SEQ), F32)
+        for line in lines:
+            same = same + jnp.where((line == chosen[k]) & earlier, 1.0, 0.0)
+        rank = jnp.sum(same, axis=1, keepdims=True).astype(jnp.int32)
+        number = chosen[k].astype(jnp.int32)
+        x = (number % SIDE - mx + SIDE) % SIDE
+        y = ((number // SIDE) % SIDE - my + SIDE) % SIDE
+        z = (number // (SIDE * SIDE) - mz + SIDE) % SIDE
+        slot = ((z * SIDE + y) * SIDE + x) * SLOTS + rank
+        codes.append(jnp.where(valid, slot * TILES, -4096))
+    lane = iota((PAD, SPREAD), 1)
+    on_lane = lane % PAD == iota((PAD, SPREAD), 0)
+    tile_of = iota((1, SPREAD), 1) // PAD
+    code_rows = [
+        jnp.sum(jnp.where(on_lane, code.astype(F32), 0.0), axis=0, keepdims=True).astype(jnp.int32)
+        + tile_of
+        for code in codes
+    ]
+    tile_down = iota((SPREAD, 1), 0) // PAD
+    code_cols = [jnp.concatenate([code] * TILES, axis=0) + tile_down for code in codes]
+
+    down_ = iota((128, 128), 0)
+    over_ = iota((128, 128), 1)
+    perm[...] = jnp.where(over_ == (down_ % 16) * TILES + down_ // 16, 1.0, 0.0).astype(BF)
+    perm_back[...] = jnp.where(down_ == (over_ % 16) * TILES + over_ // 16, 1.0, 0.0).astype(BF)
+
+    pl.semaphore_wait(bar, PEERS)
+
+    swap = pltpu.make_async_remote_copy(
+        part_ref, part_in, p_send, p_recv, device_id=sibling
+    )
+    swap.start()
+    resid[16:PAD, :] = jnp.zeros((PAD - 16, WIDTH), F32)
+    swap.wait_recv()
+    resid[:SEQ, :] = hid_ref[...].astype(F32) + (part_ref[...] + part_in[...])
+    total = resid[...]
+    scale = lax.rsqrt(jnp.mean(total * total, axis=1, keepdims=True) + EPSILON)
+    ffn_in = (total * scale * gain_ref[...].astype(F32)).astype(BF)
+
+    @pl.when(tp == 0)
+    def _():
+        rows_own[:PAD, :] = ffn_in[:, :HALF]
+
+    @pl.when(tp == 1)
+    def _():
+        rows_own[:PAD, :] = ffn_in[:, HALF:]
+
+    mine = rows_own[:PAD, :].astype(F32)
+    spread = jnp.concatenate(
+        [mine[:, c * 128 : (c + 1) * 128] for c in range(TILES)], axis=0
+    ).astype(BF)
+
+    for r in range(SIDE):
+        down = iota((PLANE, SPREAD), 0) + r * PLANE
+        hit = (down == code_rows[0]) | (down == code_rows[1]) | (down == code_rows[2])
+        rows = project(jnp.where(hit, 1.0, 0.0).astype(BF), spread).astype(BF)
+        send[r * PLANE : (r + 1) * PLANE, :] = rows
+        if r == 0:
+            recv[:ROWS, :] = rows[:ROWS, :]
+
+        @pl.loop(1 if r == 0 else 0, 16)
+        def _(j):
+            i = r * 16 + j
+            pltpu.make_async_remote_copy(
+                send.at[block(i)],
+                recv.at[block(i)],
+                d_send,
+                d_recv.at[r],
+                device_id={"ep": ahead(i)},
+            ).start()
+
+    group_exp = jnp.exp(nt_dot(ffn_in, group_ref[...]))
+    first = chosen[0].astype(jnp.int32) // GROUP_SIZE
+    in_group = iota(group_exp.shape, 1) == first
+    chosen_prob = jnp.sum(jnp.where(in_group, group_exp, 0.0), axis=1, keepdims=True) / jnp.sum(
+        group_exp, axis=1, keepdims=True
+    )
+    logits = nt_dot(ffn_in, expert_ref[...])
+    place = iota(logits.shape, 1)
+    picked = [
+        jnp.exp(
+            jnp.sum(
+                jnp.where(place == number.astype(jnp.int32), logits, 0.0), axis=1, keepdims=True
+            )
+        )
+        for number in chosen
+    ]
+    below = picked[0] + picked[1] + picked[2]
+    gates = [jnp.concatenate([chosen_prob * p / below] * TILES, axis=0) for p in picked]
+    for r in range(SIDE):
+        over = iota((SPREAD, PLANE), 1) + r * PLANE
+        weights = jnp.where(over == code_cols[0], gates[0], 0.0)
+        weights = jnp.where(over == code_cols[1], gates[1], weights)
+        weights = jnp.where(over == code_cols[2], gates[2], weights)
+        comb[:, r * PLANE : (r + 1) * PLANE] = weights.astype(BF)
+
+    def relay(source, target, r):
+        for b in range(3 * r, 3 * r + 3):
+            moved = project(perm[...], source[b * 128 : (b + 1) * 128, :]).astype(BF)
+            for c in range(TILES):
+                target[b * 16 : (b + 1) * 16, c * 128 : (c + 1) * 128] = moved[
+                    c * 16 : (c + 1) * 16, :
+                ]
+
+    def forward(r):
+        whole = pl.ds(r * PLANE, PLANE)
+        return pltpu.make_async_remote_copy(
+            recv.at[whole], recv_sib.at[whole], f_send.at[r], f_recv.at[r], device_id=sibling
+        )
+
+    def landed(buffer, sem, r):
+        low = ROWS if r == 0 else r * PLANE
+        part = buffer.at[pl.ds(low, (r + 1) * PLANE - low)]
+        return pltpu.make_async_copy(part, part, sem.at[r])
+
+    for r in range(SIDE):
+        landed(recv, d_recv, r).wait()
+        forward(r).start()
+        relay(recv, rows_own, r)
+    for load in loads:
+        load.wait()
+    for r in range(SIDE):
+        forward(r).wait_recv()
+        relay(recv_sib, rows_sib, r)
+
+    own_rows = pl.ds(pl.multiple_of(tp * HALF, HALF), HALF)
+    sib_rows = pl.ds(pl.multiple_of((1 - tp) * HALF, HALF), HALF)
+    for n in range(2):
+        cols = slice(n * 256, (n + 1) * 256)
+        gated = project(rows_own[...], wg[own_rows, cols]) + project(
+            rows_sib[...], wg[sib_rows, cols]
+        )
+        upped = project(rows_own[...], wu[own_rows, cols]) + project(
+            rows_sib[...], wu[sib_rows, cols]
+        )
+        act[:, cols] = (gated * jax.nn.sigmoid(gated) * upped).astype(BF)
+
+    y_out[...] = project(act[...], wd[:, sib_rows]).astype(BF)
+    hand = pltpu.make_async_remote_copy(y_out, y_in, s_send, s_recv, device_id=sibling)
+    hand.start()
+    y_own[...] = project(act[...], wd[:, own_rows])
+    hand.wait_recv()
+
+    for r in range(SIDE):
+        for b in range(3 * r, 3 * r + 3):
+            lines_ = slice(b * 16, (b + 1) * 16)
+            summed = (y_own[lines_, :] + y_in[lines_, :].astype(F32)).astype(BF)
+            stacked = jnp.concatenate(
+                [summed[:, c * 128 : (c + 1) * 128] for c in range(TILES)], axis=0
+            )
+            rows = project(perm_back[...], stacked).astype(BF)
+            back[b * 128 : (b + 1) * 128, :] = rows
+            if b == 0:
+                ret[:ROWS, :] = rows[:ROWS, :]
+
+        @pl.loop(1 if r == 0 else 0, 16)
+        def _(j):
+            i = r * 16 + j
+            pltpu.make_async_remote_copy(
+                back.at[block(i)],
+                ret.at[block(i)],
+                r_send,
+                r_recv.at[r],
+                device_id={"ep": behind(i)},
+            ).start()
+
+    merged = None
+    for r in range(SIDE):
+        landed(ret, r_recv, r).wait()
+        cols = slice(r * PLANE, (r + 1) * PLANE)
+        term = project(comb[:, cols], ret[cols, :])
+        merged = term if merged is None else merged + term
+    half = resid[:, own_rows]
+    for c in range(TILES):
+        cols = slice(c * 128, (c + 1) * 128)
+        line = half[:, cols] + merged[c * PAD : (c + 1) * PAD, :]
+        out_ref[:, cols] = line[:SEQ, :].astype(BF)
+
+    swap.wait_send()
+    hand.wait_send()
+    for r in range(SIDE):
+        forward(r).wait_send()
+    sent = send.at[pl.ds(ROWS, TOTAL - ROWS)]
+    pltpu.make_async_copy(sent, sent, d_send).wait()
+    gone = back.at[pl.ds(ROWS, TOTAL - ROWS)]
+    pltpu.make_async_copy(gone, gone, r_send).wait()
+
+
+def moe(partial_sum, hidden, gain, group_t, expert_t, choice_t, w_gate, w_up, w_down):
+    vmem = pl.BlockSpec(memory_space=pltpu.VMEM)
+    anywhere = pl.BlockSpec(memory_space=pl.ANY)
+    dma = pltpu.SemaphoreType.DMA
+    slots = PEERS * SLOTS
+    return pl.pallas_call(
+        moe_kernel,
+        out_shape=jax.ShapeDtypeStruct((SEQ, HALF), BF),
+        in_specs=[vmem] * 6 + [anywhere] * 3,
+        out_specs=vmem,
+        scratch_shapes=[
+            pltpu.VMEM((WIDTH, HIDDEN), BF),
+            pltpu.VMEM((WIDTH, HIDDEN), BF),
+            pltpu.VMEM((HIDDEN, WIDTH), BF),
+            pltpu.VMEM((SEQ, WIDTH), F32),
+            pltpu.VMEM((PAD, WIDTH), F32),
+            pltpu.VMEM((TOTAL, 128), BF),
+            pltpu.VMEM((TOTAL, 128), BF),
+            pltpu.VMEM((TOTAL, 128), BF),
+            pltpu.VMEM((SPREAD, TOTAL), BF),
+            pltpu.VMEM((128, 128), BF),
+            pltpu.VMEM((128, 128), BF),
+            pltpu.VMEM((slots, HALF), BF),
+            pltpu.VMEM((slots, HALF), BF),
+            pltpu.VMEM((slots, HIDDEN), BF),
+            pltpu.VMEM((slots, HALF), F32),
+            pltpu.VMEM((slots, HALF), BF),
+            pltpu.VMEM((slots, HALF), BF),
+            pltpu.VMEM((TOTAL, 128), BF),
+            pltpu.VMEM((TOTAL, 128), BF),
+            dma((3,)),
+            dma,
+            dma,
+            dma,
+            dma((SIDE,)),
+            dma((SIDE,)),
+            dma((SIDE,)),
+            dma,
+            dma,
+            dma,
+            dma((SIDE,)),
+        ],
+        compiler_params=pltpu.CompilerParams(
+            collective_id=0, has_side_effects=True, vmem_limit_bytes=40 * 1024 * 1024
+        ),
+        name="moe",
+    )(partial_sum, hidden, gain, group_t, expert_t, choice_t, w_gate, w_up, w_down)
 
 
 def normed(values, gain):
@@ -146,46 +465,17 @@
     mixed = (grouped.reshape(seq_rows, value_width) * gain_local.astype(jnp.float32)).astype(
         jnp.bfloat16
     )
-    residual = hidden.astype(jnp.float32) + of_everyone(project(mixed, out_proj), "tp")
-    ffn_in = normed(residual, ffn_gain).astype(jnp.bfloat16)
-    group_weights = jnp.exp(project(ffn_in, group_router))
-    group_prob = group_weights / jnp.sum(group_weights, axis=1, keepdims=True)
-    group_of = expert_choice[:, 0] // GROUP_SIZE
-    group_mask = jnp.arange(group_router.shape[1])[None, :] == group_of[:, None]
-    chosen_prob = jnp.sum(jnp.where(group_mask, group_prob, 0.0), axis=1, keepdims=True)
-    picked_exp = jnp.exp(jnp.take_along_axis(project(ffn_in, expert_router), expert_choice, axis=1))
-    gates = chosen_prob * picked_exp / jnp.sum(picked_exp, axis=1, keepdims=True)
-    experts_total = expert_router.shape[1]
-    top_count = expert_choice.shape[1]
-    capacity = top_count * ((seq_rows + experts_total - 1) // experts_total)
-    flat_choice = expert_choice.reshape(-1)
-    one_hot = (flat_choice[:, None] == jnp.arange(experts_total)[None, :]).astype(jnp.int32)
-    earlier = jnp.cumsum(one_hot, axis=0) - one_hot
-    position = jnp.sum(earlier * one_hot, axis=1)
-    target = (flat_choice * capacity + position).reshape(seq_rows, top_count)
-    routing = target[:, :, None] == jnp.arange(experts_total * capacity)[None, None, :]
-    dispatch = jnp.any(routing, axis=1).T.astype(jnp.bfloat16)
-    combine = jnp.sum(routing.astype(jnp.float32) * gates[:, :, None], axis=1)
-    model_width = ffn_in.shape[1]
-    half_width = model_width // tp_count
-    own_columns = lax.dynamic_slice_in_dim(ffn_in, tp_index * half_width, half_width, 1)
-    outgoing = (
-        project(dispatch, own_columns).astype(jnp.bfloat16).reshape(ep_count, capacity, half_width)
-    )
-    arrived = gathered_copies(
-        lax.all_to_all(outgoing, "ep", split_axis=0, concat_axis=0, tiled=True), "tp", 2
-    )
-    slot_total = arrived.shape[1]
-    flat_rows = arrived.reshape(-1, model_width)
-    activated = (
-        jax.nn.silu(project(flat_rows, expert_gate[0])) * project(flat_rows, expert_up[0])
-    ).astype(jnp.bfloat16)
-    partial_value = project(activated, expert_down[0]).reshape(ep_count, slot_total, model_width)
-    reduced = sum_at_owner(partial_value.astype(jnp.bfloat16), "tp", 2).astype(jnp.bfloat16)
-    returned = lax.all_to_all(reduced, "ep", split_axis=0, concat_axis=0, tiled=True)
-    expert_sum = jnp.dot(combine, returned.reshape(-1, half_width).astype(jnp.float32))
-    residual_half = lax.dynamic_slice_in_dim(residual, tp_index * half_width, half_width, 1)
-    layer_out = (residual_half + expert_sum).astype(jnp.bfloat16)
+    layer_out = moe(
+        project(mixed, out_proj),
+        hidden,
+        ffn_gain.reshape(1, -1),
+        group_router.T,
+        expert_router.T,
+        expert_choice.T,
+        expert_gate[0],
+        expert_up[0],
+        expert_down[0],
+    )
     return (layer_out, new_state)
 
 

time: 93.2 us -> 62.2 us (0.67)
  Pallas kernels: 0 us -> 34.2 us
  waiting for transfers between devices: 22.8 us -> 0 us
  starting transfers between devices: 20.7 us -> 0 us
  blocking collectives: 10.4 us -> 0 us
  local copies, waits for them, and re-layouts: 11.7 us -> 5.58 us
  matrix products: 15.1 us -> 11.1 us
    pallas_call x0 -> x1, Pallas kernels: none -> 34.2 us  [moe(): pl.pallas_call(moe_kernel, out_shape=jax.ShapeDtypeStruct((SEQ, HALF), BF...]
    all_to_all x3 -> x0, waiting for transfers between devices: 22.8 us -> none  [the longest x1 12.5 us: on_device(): lax.all_to_all(reduced, 'ep', split_axis=0, concat_axis=0, tiled=True)]
    all_to_all x3 -> x0, starting transfers between devices: 20.7 us -> none  [the longest x1 11.2 us: on_device(): lax.all_to_all(outgoing, 'ep', split_axis=0, concat_axis=0, tiled=True)]
    all_to_all x2 -> x0, blocking collectives: 10.4 us -> none  [the longest x1 6.01 us: sent_to_all(): lax.all_to_all(jnp.broadcast_to(array[None], (peers, *array.shape)), axis...]
    dot_general x12 -> x6, matrix products: 12.7 us -> 6.87 us  [project(): return jnp.dot(left, right, preferred_element_type=jnp.float32)]
    unnamed x22 -> x39, local copies, waits for them, and re-layouts: 2.03 us -> 4.81 us
    dot_general x1, matrix products: 1.6 us -> 4.22 us  [on_device(): jnp.einsum('thpn,thn->thp', new_state, heads_read)]
    add x1, other arithmetic: 4.56 us -> 6.69 us  [on_device(): decay[:, :, None, None] * scan_state]
  transfers between devices with their start and end apart: 3 -> 0, of which waited for: 3 -> 0; matrix products, arithmetic and copies ran while one was open for 4% -> 0% of each run, Pallas kernels for 0% -> 0%
where the time goes in v1:
time: 62.2 us; the launch traced here: 61.7 us
  Pallas kernels  34.2 us (55%)
  matrix products  11.1 us (18%)
  other arithmetic  9.86 us (16%)
  local copies, waits for them, and re-layouts  5.58 us (9%)
  between operations  0.95 us (2%)
    pallas_call x1, Pallas kernels, moe(): pl.pallas_call(moe_kernel, out_shape=jax.ShapeDtypeStruct((SEQ, HALF), BF...  34.2 us
    dot_general x6, matrix products, project(): return jnp.dot(left, right, preferred_element_type=jnp.float32)  6.87 us
    add x1, other arithmetic, on_device(): decay[:, :, None, None] * scan_state  6.69 us
    unnamed x39, local copies, waits for them, and re-layouts  4.81 us
    dot_general x1, matrix products, on_device(): jnp.einsum('thpn,thn->thp', new_state, heads_read)  4.22 us

profile of v1, /device:TPU:1, one launch (start us, length us, event | category | flops | bytes accessed | tf_op | source)
XLA Modules:
  0.0 61.7 jit_solution(3925763198297428496)
XLA Ops:
  0.7 0.9 %dynamic-slice_convert_fusion.3 = (f32[1,512]{1,0:T(1,128)S(1)}, f32[1,512]{1,0:T(1,128)S(1)}, f32[1,512]{1,0:T(1,128)S(1)}, f32[1,512]{1,0:T(1,128)S(1)}) fusion(bf16[4,1024]{1,0:T(4,128)(2,1)} %param.36, s32[]{:T(128)S(6)} %add.116, s32[]{:T(128)S(6)} %select_n.20, s32[]{:T(128)S(6)} %add.117, s32[]{:T(128)S(6)} %add.118), kind=kLoop, calls=%fused_computation.52 | loop fusion | flops 2048 | bytes 12304 | tf_op jit(solution)/shard_map/mul | solution.py:372
  1.7 0.7 %convert_element_type.118 = f32[2048]{0:T(1024)S(1)} convert(bf16[2048]{0:T(1024)(128)(2,1)} %param.27) | non-fusion elementwise | flops 2048 | bytes 12288 | tf_op jit(solution)/shard_map/convert_element_type | solution.py:368
  2.4 1.0 %fusion.16 = f32[22]{0:T(128)S(1)} fusion(bf16[22,2048]{1,0:T(8,128)(2,1)} %hid_ref.1), kind=kLoop, calls=%fused_computation.24 | loop fusion | flops 135146 | bytes 90200 | tf_op jit(solution)/shard_map/reduce_sum | solution.py:367
  3.4 2.1 %divide_multiply_fusion = f32[22,512]{1,0:T(8,128)S(1)} fusion(bf16[2048,512]{1,0:T(8,128)(2,1)} %param.29, bf16[22,3,512]{2,0,1:T(8,128)(2,1)} %param.39, f32[512]{0:T(512)S(1)} %bitcast.77, f32[512]{0:T(512)S(1)} %bitcast.75, f32[512]{0:T(512)S(1)} %bitcast.76, f32[512]{0:T(512)S(1)} %bitcast.74, bf16[22,2048]{1,0:T(8,128)(2,1)} %hid_ref.1, ...), kind=kOutput, calls=%fused_computation.33 | convolution fusion | flops 46497792 | bytes 2316376 | tf_op jit(solution)/shard_map/dot_general | solution.py:381
  5.8 0.2 multiply_exponential_fusion
  6.0 0.1 copy.29
  6.1 0.1 broadcast_multiply_fusion
  6.2 0.1 dynamic-slice_convert_fusion.7
  6.3 1.1 %divide_multiply_fusion.2 = f32[22,256]{1,0:T(8,128)S(1)} fusion(bf16[2048,256]{1,0:T(8,128)(2,1)S(1)} %copy-done.8, bf16[22,3,256]{2,0,1:T(8,128)(2,1)} %param.40, f32[256]{0:T(256)S(1)} %bitcast.82, f32[256]{0:T(256)S(1)} %bitcast.84, f32[256]{0:T(256)S(1)} %bitcast.83, f32[256]{0:T(256)S(1)} %bitcast.85, bf16[22,2048]{1,0:T(8,128)(2,1)S(1)} %copy-done.1, ...), kind=kOutput, calls=%fused_computation.45 | convolution fusion | flops 23339008 | bytes 1207384 | tf_op jit(solution)/shard_map/dot_general | solution.py:381
  7.4 0.1 copy.28
  7.5 6.7 %multiply_add_fusion = f32[22,8,64,128]{3,2,1,0:T(8,128)} fusion(f32[22,8,64,128]{3,2,1,0:T(8,128)} %param.42, f32[22,8,128]{2,1,0:T(8,128)S(1)} %bitcast.69, f32[22,8,64]{2,1,0:T(8,128)S(1)} %broadcast_multiply_fusion, f32[22,8]{1,0:T(8,128)S(1)} %copy.28), kind=kLoop, calls=%fused_computation | loop fusion | flops 4325376 | bytes 11670208 | tf_op jit(solution)/shard_map/add | solution.py:455
  14.2 1.1 %divide_multiply_fusion.1 = f32[22,256]{1,0:T(8,128)S(1)} fusion(bf16[2048,256]{1,0:T(8,128)(2,1)S(1)} %copy-done.9, bf16[22,3,256]{2,0,1:T(8,128)(2,1)} %param.41, f32[256]{0:T(256)S(1)} %bitcast.81, f32[256]{0:T(256)S(1)} %bitcast.79, f32[256]{0:T(256)S(1)} %bitcast.80, f32[256]{0:T(256)S(1)} %bitcast.78, bf16[22,2048]{1,0:T(8,128)(2,1)S(1)} %copy-done.1, ...), kind=kOutput, calls=%fused_computation.44 | convolution fusion | flops 23339008 | bytes 1207384 | tf_op jit(solution)/shard_map/dot_general | solution.py:381
  15.3 4.2 %fusion.31 = f32[22,8,1,64]{3,2,1,0:T(1,128)S(1)} fusion(f32[22,8,64,128]{3,2,1,0:T(8,128)} %multiply_add_fusion, f32[22,8,128,1]{2,3,1,0:T(1,128)S(1)} %bitcast.71), kind=kOutput, calls=%fused_computation.66 | convolution fusion | flops 2883584 | bytes 5902336 | tf_op jit(solution)/shard_map/thpn,thn->thp/dot_general | solution.py:459
  19.6 0.1 dynamic_slice.30
  19.7 0.1 reshape.77
  19.9 2.1 %fusion.30 = (f32[22,512]{1,0:T(8,128)S(1)}, f32[22,512]{1,0:T(8,128)S(1)}) fusion(f32[22,512]{1,0:T(8,128)S(1)} %reshape.77, bf16[2048,512]{1,0:T(8,128)(2,1)} %param.28, bf16[22,2048]{1,0:T(8,128)(2,1)S(1)} %copy-done.1, f32[2048]{0:T(1024)S(1)} %convert_element_type.118, f32[22]{0:T(128)S(1)} %add_rsqrt_fusion.1), kind=kOutput, calls=%fused_computation.65 | convolution fusion | flops 46407680 | bytes 2330712 | tf_op jit(solution)/shard_map/dot_general | solution.py:381
  22.0 0.1 reduce_sum.19
  22.1 0.1 mul.354
  22.3 0.4 fusion.20.part_ref
  22.8 0.9 %copy-done.2 = bf16[1,2048,512]{2,1,0:T(8,128)(2,1)S(1)} copy-done((bf16[1,2048,512]{2,1,0:T(8,128)(2,1)S(1)}, bf16[1,2048,512]{2,1,0:T(8,128)(2,1)}, u32[]{:S(2)}) %copy-start.2) | copy-done | bytes 2097176
  23.7 1.6 %copy-done.3 = bf16[1,2048,512]{2,1,0:T(8,128)(2,1)S(1)} copy-done((bf16[1,2048,512]{2,1,0:T(8,128)(2,1)S(1)}, bf16[1,2048,512]{2,1,0:T(8,128)(2,1)}, u32[]{:S(2)}) %copy-start.3) | copy-done | bytes 2097176
  25.3 1.6 %copy-done.4 = bf16[1,512,2048]{2,1,0:T(8,128)(2,1)S(1)} copy-done((bf16[1,512,2048]{2,1,0:T(8,128)(2,1)S(1)}, bf16[1,512,2048]{2,1,0:T(8,128)(2,1)}, u32[]{:S(2)}) %copy-start.4) | copy-done | bytes 2097176
  26.9 34.2 %moe.1 = bf16[22,1024]{1,0:T(8,128)(2,1)S(1)} custom-call(f32[22,2048]{1,0:T(8,128)S(1)} %fusion.20.part_ref, bf16[22,2048]{1,0:T(8,128)(2,1)S(1)} %copy-done.1, bf16[1,2048]{1,0:T(2,128)(2,1)S(1)} %reshape.78.gain_ref, bf16[8,2048]{1,0:T(8,128)(2,1)S(1)} %bitcast.67, bf16[64,2048]{1,0:T(8,128)(2,1)S(1)} %bitcast.66, s32[3,22]{1,0:T(4,128)S(1)} %bitcast.68, ...), custom_call_target="tpu_custom_call" | custom-call | tf_op jit(solution)/shard_map/moe/pallas_call | solution.py:321
  61.1 0.6 %copy.34 = bf16[22,1024]{1,0:T(8,128)(2,1)} copy(bf16[22,1024]{1,0:T(8,128)(2,1)S(1)} %moe.1) | data formatting | bytes 90112
  (48 shorter events, 0.6 us)
Async XLA Ops:
  0.6 21.7 %copy-start = (bf16[512,2048]{1,0:T(8,128)(2,1)S(1)}, bf16[512,2048]{1,0:T(8,128)(2,1)}, u32[]{:S(2)}) copy-start(bf16[512,2048]{1,0:T(8,128)(2,1)} %param.44) | copy-start | bytes 6291460
  0.6 5.1 %copy-start.1 = (bf16[22,2048]{1,0:T(8,128)(2,1)S(1)}, bf16[22,2048]{1,0:T(8,128)(2,1)}, u32[]{:S(2)}) copy-start(bf16[22,2048]{1,0:T(8,128)(2,1)} %hid_ref.1) | copy-start | bytes 270340
  0.7 4.9 %copy-start.15 = (f32[16]{0:T(128)S(1)}, f32[16]{0:T(128)}, u32[]{:S(2)}) copy-start(f32[16]{0:T(128)} %param.34) | copy-start | bytes 196
  0.7 5.0 %copy-start.16 = (f32[16]{0:T(128)S(1)}, f32[16]{0:T(128)}, u32[]{:S(2)}) copy-start(f32[16]{0:T(128)} %param.33) | copy-start | bytes 196
  0.7 5.1 %copy-start.14 = (bf16[2048,16]{0,1:T(8,128)(2,1)S(1)}, bf16[2048,16]{0,1:T(8,128)(2,1)}, u32[]{:S(2)}) copy-start(bf16[2048,16]{0,1:T(8,128)(2,1)} %param.32) | copy-start | bytes 196612
  0.7 5.5 %copy-start.12 = (bf16[4,512]{1,0:T(4,128)(2,1)S(1)}, bf16[4,512]{1,0:T(4,128)(2,1)}, u32[]{:S(2)}) copy-start(bf16[4,512]{1,0:T(4,128)(2,1)} %param.37) | copy-start | bytes 12292
  0.7 5.5 %copy-start.11 = (bf16[4,512]{1,0:T(4,128)(2,1)S(1)}, bf16[4,512]{1,0:T(4,128)(2,1)}, u32[]{:S(2)}) copy-start(bf16[4,512]{1,0:T(4,128)(2,1)} %param.38) | copy-start | bytes 12292
  0.7 5.6 %copy-start.8 = (bf16[2048,256]{1,0:T(8,128)(2,1)S(1)}, bf16[2048,256]{1,0:T(8,128)(2,1)}, u32[]{:S(2)}) copy-start(bf16[2048,256]{1,0:T(8,128)(2,1)} %param.30) | copy-start | bytes 3145732
  7.5 6.7 %copy-start.9 = (bf16[2048,256]{1,0:T(8,128)(2,1)S(1)}, bf16[2048,256]{1,0:T(8,128)(2,1)}, u32[]{:S(2)}) copy-start(bf16[2048,256]{1,0:T(8,128)(2,1)} %param.31) | copy-start | bytes 3145732
  15.3 4.2 %copy-start.17 = (f32[16]{0:T(128)S(1)}, f32[16]{0:T(128)}, u32[]{:S(2)}) copy-start(f32[16]{0:T(128)} %param.35) | copy-start | bytes 196
  19.5 2.7 %copy-start.13 = (bf16[1024]{0:T(1024)(128)(2,1)S(1)}, bf16[1024]{0:T(1024)(128)(2,1)}, u32[]{:S(2)}) copy-start(bf16[1024]{0:T(1024)(128)(2,1)} %param.43) | copy-start | bytes 6148
  19.8 2.9 %copy-start.10 = (bf16[2048]{0:T(1024)(128)(2,1)S(1)}, bf16[2048]{0:T(1024)(128)(2,1)}, u32[]{:S(2)}) copy-start(bf16[2048]{0:T(1024)(128)(2,1)} %param.45) | copy-start | bytes 12292
  19.8 2.9 %copy-start.5 = (bf16[2048,64]{0,1:T(8,128)(2,1)S(1)}, bf16[2048,64]{0,1:T(8,128)(2,1)}, u32[]{:S(2)}) copy-start(bf16[2048,64]{0,1:T(8,128)(2,1)} %param.47) | copy-start | bytes 786436
  19.8 2.9 %copy-start.6 = (bf16[2048,8]{0,1:T(8,128)(2,1)S(1)}, bf16[2048,8]{0,1:T(8,128)(2,1)}, u32[]{:S(2)}) copy-start(bf16[2048,8]{0,1:T(8,128)(2,1)} %param.46) | copy-start | bytes 98308
  19.8 2.9 %copy-start.7 = (s32[22,3]{0,1:T(4,128)S(1)}, s32[22,3]{0,1:T(4,128)}, u32[]{:S(2)}) copy-start(s32[22,3]{0,1:T(4,128)} %param.48) | copy-start | bytes 796
  22.1 1.6 %copy-start.2 = (bf16[1,2048,512]{2,1,0:T(8,128)(2,1)S(1)}, bf16[1,2048,512]{2,1,0:T(8,128)(2,1)}, u32[]{:S(2)}) copy-start(bf16[1,2048,512]{2,1,0:T(8,128)(2,1)} %param.49) | copy-start | bytes 6291460
  23.7 1.6 %copy-start.3 = (bf16[1,2048,512]{2,1,0:T(8,128)(2,1)S(1)}, bf16[1,2048,512]{2,1,0:T(8,128)(2,1)}, u32[]{:S(2)}) copy-start(bf16[1,2048,512]{2,1,0:T(8,128)(2,1)} %param.50) | copy-start | bytes 6291460
  25.3 1.6 %copy-start.4 = (bf16[1,512,2048]{2,1,0:T(8,128)(2,1)S(1)}, bf16[1,512,2048]{2,1,0:T(8,128)(2,1)}, u32[]{:S(2)}) copy-start(bf16[1,512,2048]{2,1,0:T(8,128)(2,1)} %param.51) | copy-start | bytes 6291460

commit v2 on v1

--- a/solution.py
+++ b/solution.py
@@ -6,11 +6,7 @@
 from jax.sharding import PartitionSpec as P
 
 GROUP_SIZE = 8
-
-
 EPSILON = 1e-06
-
-
 SIDE = 4
 PEERS = 64
 SLOTS = 3
@@ -24,6 +20,12 @@
 SEQ = 22
 PAD = 24
 SPREAD = TILES * PAD
+HEADS = 8
+HEAD_DIM = 64
+VECTOR = 256
+PAIR = 2 * HIDDEN
+PAIRS = SEQ // 2
+VMEM_ALL = 67043328
 BF = jnp.bfloat16
 F32 = jnp.float32
 
@@ -40,48 +42,231 @@
     return lax.broadcasted_iota(jnp.int32, shape, dim)
 
 
-def moe_kernel(
-    part_ref,
-    hid_ref,
-    gain_ref,
-    group_ref,
-    expert_ref,
-    choice_ref,
-    gate_hbm,
-    up_hbm,
-    down_hbm,
-    out_ref,
-    wg,
-    wu,
-    wd,
-    part_in,
-    resid,
-    send,
-    recv,
-    recv_sib,
-    comb,
-    perm,
-    perm_back,
-    rows_own,
-    rows_sib,
-    act,
-    y_own,
-    y_out,
-    y_in,
-    back,
-    ret,
-    w_sem,
-    p_send,
-    p_recv,
-    d_send,
-    d_recv,
-    f_send,
-    f_recv,
-    s_send,
-    s_recv,
-    r_send,
-    r_recv,
-):
+def mix_kernel(*refs):
+    sources, (normed_ref, mixed_ref, state_out) = refs[:16], refs[16:19]
+    state_hbm, held = sources[-1], refs[19:34]
+    state_ref, left, left_t, right, read_t, decays, acc, load_sem, in_sem, out_sem = refs[34:]
+    (
+        hid_ref,
+        gain_ref,
+        step_ref,
+        bias_ref,
+        rate_ref,
+        skip_ref,
+        value_ref,
+        write_ref,
+        read_ref,
+        value_taps_ref,
+        write_taps_ref,
+        read_taps_ref,
+        value_tail_ref,
+        write_tail_ref,
+        read_tail_ref,
+    ) = held
+    tp = lax.axis_index("tp")
+
+    def rows_of(c):
+        return pl.ds(pl.multiple_of(c * PAIR, PAIR), PAIR)
+
+    def chunk(c):
+        rows = rows_of(c)
+        return pltpu.make_async_copy(state_hbm.at[rows], state_ref.at[rows], in_sem.at[c])
+
+    def chunk_out(c):
+        rows = rows_of(c)
+        return pltpu.make_async_copy(state_ref.at[rows], state_out.at[rows], out_sem.at[c])
+
+    loads = [
+        pltpu.make_async_copy(sources[n], held[n], load_sem.at[n]) for n in range(len(held))
+    ]
+    for load in loads:
+        load.start()
+    for c in range(PAIRS):
+        chunk(c).start()
+    for load in loads[:6]:
+        load.wait()
+
+    wide = hid_ref[...].astype(F32)
+    scale = lax.rsqrt(jnp.mean(wide * wide, axis=1, keepdims=True) + EPSILON)
+    mixer_in = (wide * scale * gain_ref[...].astype(F32).reshape(1, WIDTH)).astype(BF)
+    normed_ref[...] = mixer_in
+
+    def local_heads(line):
+        return jnp.where(tp == 0, line[:, :HEADS], line[:, HEADS:])
+
+    bias = local_heads(bias_ref[...])
+    rate = jnp.exp(local_heads(rate_ref[...]))
+    skip = local_heads(skip_ref[...])
+    raw = local_heads(nt_dot(mixer_in, step_ref[...])) + bias
+    step = jnp.maximum(raw, 0.0) + jnp.log1p(jnp.exp(-jnp.abs(raw)))
+    decay = jnp.exp(-step * rate)
+    for h in range(HEADS):
+        decays[:SEQ, h, :] = jnp.broadcast_to(decay[:, h : h + 1], (SEQ, 128))
+
+    def convolve(tail_ref, newest, taps_ref, width):
+        cols = pl.ds(pl.multiple_of(tp * width, width), width)
+        taps = taps_ref[:, cols].astype(F32)
+        summed = taps[3:4, :] * newest.astype(BF).astype(F32)
+        for offset in range(3):
+            summed = summed + taps[offset : offset + 1, :] * tail_ref[offset].astype(F32)
+        return summed * jax.nn.sigmoid(summed)
+
+    for load in loads[6:]:
+        load.wait()
+    value = convolve(value_tail_ref, project(mixer_in, value_ref[...]), value_taps_ref, HIDDEN)
+    write = convolve(write_tail_ref, project(mixer_in, write_ref[...]), write_taps_ref, VECTOR)
+    read = convolve(read_tail_ref, project(mixer_in, read_ref[...]), read_taps_ref, VECTOR)
+
+    head_of = iota((1, HIDDEN), 1) // HEAD_DIM
+    step_wide = jnp.zeros((SEQ, HIDDEN), F32)
+    skip_wide = jnp.zeros((1, HIDDEN), F32)
+    for h in range(HEADS):
+        step_wide = jnp.where(head_of == h, step[:, h : h + 1], step_wide)
+        skip_wide = jnp.where(head_of == h, skip[:, h : h + 1], skip_wide)
+    drive = step_wide * value
+
+    drive_high = drive.astype(BF).astype(F32)
+    write_high = write.astype(BF).astype(F32)
+    left[...] = jnp.zeros((128, HIDDEN), F32)
+    left[:SEQ, :] = drive_high
+    left[32 : 32 + SEQ, :] = drive_high
+    left[64 : 64 + SEQ, :] = drive - drive_high
+    right[...] = jnp.zeros((128, VECTOR), F32)
+    right[:SEQ, :] = write_high
+    right[32 : 32 + SEQ, :] = write - write_high
+    right[64 : 64 + SEQ, :] = write_high
+    for b in range(HIDDEN // 128):
+        part = slice(b * 128, (b + 1) * 128)
+        left_t[part, :] = left[:, part].T.astype(BF)
+    left[:, :VECTOR] = jnp.zeros((128, VECTOR), F32)
+    left[:SEQ, :VECTOR] = read
+    for g in range(2):
+        part = slice(g * 128, (g + 1) * 128)
+        read_t[part, :] = left[:, part].T
+    acc[...] = jnp.zeros((HIDDEN, 128), F32)
+
+    stacked_row = iota((128, 128), 0) % 32
+    lane = iota((128, 128), 1)
+
+    @pl.loop(0, PAIRS)
+    def _(c):
+        chunk(c).wait()
+        for g in range(2):
+            part = slice(g * 128, (g + 1) * 128)
+            pair = [2 * c, 2 * c + 1]
+            outer = project(
+                left_t[g * 256 : (g + 1) * 256, :],
+                jnp.concatenate(
+                    [jnp.where(stacked_row == t, right[:, part], 0.0) for t in pair], axis=1
+                ).astype(BF),
+            )
+            fresh = []
+            for k in range(2):
+                pieces = []
+                for h in range(4):
+                    rows = pl.ds(
+                        pl.multiple_of(c * PAIR + k * HIDDEN + g * 256 + h * HEAD_DIM, HEAD_DIM),
+                        HEAD_DIM,
+                    )
+                    keep = decays[2 * c + k, g * 4 + h : g * 4 + h + 1, :]
+                    new = (
+                        keep * state_ref[rows, :]
+                        + outer[h * HEAD_DIM : (h + 1) * HEAD_DIM, k * 128 : (k + 1) * 128]
+                    )
+                    state_ref[rows, :] = new
+                    pieces.append(new.astype(BF))
+                fresh.append(jnp.concatenate(pieces, axis=0))
+            reader = jnp.concatenate(
+                [jnp.where(lane == t, read_t[part, :], 0.0) for t in pair], axis=0
+            ).astype(BF)
+            acc[g * 256 : (g + 1) * 256, :] += project(jnp.concatenate(fresh, axis=1), reader)
+        chunk_out(c).start()
+
+    for b in range(HIDDEN // 128):
+        part = slice(b * 128, (b + 1) * 128)
+        mixed_ref[:, part] = acc[part, :].T[:SEQ, :] + skip_wide[:, part] * value[:, part]
+
+    for c in range(PAIRS):
+        chunk_out(c).wait()
+
+
+def mix(*operands):
+    vmem = pl.BlockSpec(memory_space=pltpu.VMEM)
+    hbm = pl.BlockSpec(memory_space=pltpu.HBM)
+    dma = pltpu.SemaphoreType.DMA
+    return pl.pallas_call(
+        mix_kernel,
+        out_shape=(
+            jax.ShapeDtypeStruct((SEQ, WIDTH), BF),
+            jax.ShapeDtypeStruct((SEQ, HIDDEN), F32),
+            jax.ShapeDtypeStruct((SEQ * HIDDEN, 128), F32),
+        ),
+        in_specs=[hbm] * len(operands),
+        out_specs=(vmem, vmem, hbm),
+        scratch_shapes=[pltpu.VMEM(x.shape, x.dtype) for x in operands]
+        + [
+            pltpu.VMEM((128, HIDDEN), F32),
+            pltpu.VMEM((HIDDEN, 128), BF),
+            pltpu.VMEM((128, VECTOR), F32),
+            pltpu.VMEM((VECTOR, 128), F32),
+            pltpu.VMEM((PAD, HEADS, 128), F32),
+            pltpu.VMEM((HIDDEN, 128), F32),
+            dma((len(operands) - 1,)),
+            dma((PAIRS,)),
+            dma((PAIRS,)),
+        ],
+        compiler_params=pltpu.CompilerParams(vmem_limit_bytes=VMEM_ALL),
+        name="mix",
+    )(*operands)
+
+
+def moe_kernel(*refs):
+    sources, out_ref, held = refs[:13], refs[13], refs[14:27]
+    (
+        normed_ref,
+        gate_proj,
+        heads_ref,
+        group_gain_ref,
+        out_proj,
+        hid_ref,
+        gain_ref,
+        group_ref,
+        expert_ref,
+        choice_ref,
+        wg,
+        wu,
+        wd,
+    ) = held
+    (
+        part_ref,
+        part_in,
+        resid,
+        send,
+        recv,
+        recv_sib,
+        comb,
+        perm,
+        perm_back,
+        rows_own,
+        rows_sib,
+        act,
+        y_own,
+        y_out,
+        y_in,
+        back,
+        ret,
+        w_sem,
+        p_send,
+        p_recv,
+        d_send,
+        d_recv,
+        f_send,
+        f_recv,
+        s_send,
+        s_recv,
+        r_send,
+        r_recv,
+    ) = refs[27:]
     me = lax.axis_index("ep")
     tp = lax.axis_index("tp")
     mx, my, mz = me % SIDE, (me // SIDE) % SIDE, me // (SIDE * SIDE)
@@ -103,6 +288,12 @@
     def block(i):
         return pl.ds(pl.multiple_of(i * ROWS, TILES), ROWS)
 
+    loads = [
+        pltpu.make_async_copy(sources[n], held[n], w_sem.at[n]) for n in range(len(held))
+    ]
+    for n in [9, 0, 1, 2, 3, 4, 5, 6, 7, 8, 10, 11, 12]:
+        loads[n].start()
+
     bar = pltpu.get_barrier_semaphore()
     pl.semaphore_signal(bar, inc=1, device_id=sibling)
 
@@ -110,14 +301,7 @@
     def _(i):
         pl.semaphore_signal(bar, inc=1, device_id={"ep": ahead(i)})
 
-    loads = [
-        pltpu.make_async_copy(gate_hbm, wg, w_sem.at[0]),
-        pltpu.make_async_copy(up_hbm, wu, w_sem.at[1]),
-        pltpu.make_async_copy(down_hbm, wd, w_sem.at[2]),
-    ]
-    for load in loads:
-        load.start()
-
+    loads[9].wait()
     diagonal = iota((PAD, SEQ), 0) == iota((PAD, SEQ), 1)
     earlier = iota((PAD, SEQ), 1) < iota((PAD, SEQ), 0)
     valid = iota((PAD, 1), 0) < SEQ
@@ -151,18 +335,36 @@
     perm[...] = jnp.where(over_ == (down_ % 16) * TILES + down_ // 16, 1.0, 0.0).astype(BF)
     perm_back[...] = jnp.where(down_ == (over_ % 16) * TILES + over_ // 16, 1.0, 0.0).astype(BF)
 
+    for load in loads[:4]:
+        load.wait()
+    gate = project(normed_ref[...], gate_proj[...]).astype(BF).astype(F32)
+    gated = heads_ref[...] * (gate * jax.nn.sigmoid(gate))
+    mixer_cols = pl.ds(pl.multiple_of(tp * HIDDEN, HIDDEN), HIDDEN)
+    group_gain = group_gain_ref[mixer_cols].astype(F32).reshape(1, HIDDEN)
+    mixed = []
+    for g in range(2):
+        cols = slice(g * 256, (g + 1) * 256)
+        part = gated[:, cols]
+        spread_ = lax.rsqrt(jnp.mean(part * part, axis=1, keepdims=True) + EPSILON)
+        mixed.append(part * spread_ * group_gain[:, cols])
+    mixed = jnp.concatenate(mixed, axis=1).astype(BF)
+    loads[4].wait()
+    part_ref[...] = project(mixed, out_proj[...])
+
     pl.semaphore_wait(bar, PEERS)
 
     swap = pltpu.make_async_remote_copy(
         part_ref, part_in, p_send, p_recv, device_id=sibling
     )
     swap.start()
+    for load in loads[5:9]:
+        load.wait()
     resid[16:PAD, :] = jnp.zeros((PAD - 16, WIDTH), F32)
     swap.wait_recv()
     resid[:SEQ, :] = hid_ref[...].astype(F32) + (part_ref[...] + part_in[...])
     total = resid[...]
     scale = lax.rsqrt(jnp.mean(total * total, axis=1, keepdims=True) + EPSILON)
-    ffn_in = (total * scale * gain_ref[...].astype(F32)).astype(BF)
+    ffn_in = (total * scale * gain_ref[...].astype(F32).reshape(1, WIDTH)).astype(BF)
 
     @pl.when(tp == 0)
     def _():
@@ -244,7 +446,7 @@
         landed(recv, d_recv, r).wait()
         forward(r).start()
         relay(recv, rows_own, r)
-    for load in loads:
+    for load in loads[10:]:
         load.wait()
     for r in range(SIDE):
         forward(r).wait_recv()
@@ -313,20 +515,19 @@
     pltpu.make_async_copy(gone, gone, r_send).wait()
 
 
-def moe(partial_sum, hidden, gain, group_t, expert_t, choice_t, w_gate, w_up, w_down):
+def moe(*operands):
     vmem = pl.BlockSpec(memory_space=pltpu.VMEM)
-    anywhere = pl.BlockSpec(memory_space=pl.ANY)
+    hbm = pl.BlockSpec(memory_space=pltpu.HBM)
     dma = pltpu.SemaphoreType.DMA
     slots = PEERS * SLOTS
     return pl.pallas_call(
         moe_kernel,
         out_shape=jax.ShapeDtypeStruct((SEQ, HALF), BF),
-        in_specs=[vmem] * 6 + [anywhere] * 3,
+        in_specs=[hbm] * len(operands),
         out_specs=vmem,
-        scratch_shapes=[
-            pltpu.VMEM((WIDTH, HIDDEN), BF),
-            pltpu.VMEM((WIDTH, HIDDEN), BF),
-            pltpu.VMEM((HIDDEN, WIDTH), BF),
+        scratch_shapes=[pltpu.VMEM(x.shape, x.dtype) for x in operands]
+        + [
+            pltpu.VMEM((SEQ, WIDTH), F32),
             pltpu.VMEM((SEQ, WIDTH), F32),
             pltpu.VMEM((PAD, WIDTH), F32),
             pltpu.VMEM((TOTAL, 128), BF),
@@ -343,7 +544,7 @@
             pltpu.VMEM((slots, HALF), BF),
             pltpu.VMEM((TOTAL, 128), BF),
             pltpu.VMEM((TOTAL, 128), BF),
-            dma((3,)),
+            dma((len(operands),)),
             dma,
             dma,
             dma,
@@ -356,29 +557,10 @@
             dma((SIDE,)),
         ],
         compiler_params=pltpu.CompilerParams(
-            collective_id=0, has_side_effects=True, vmem_limit_bytes=40 * 1024 * 1024
+            collective_id=0, has_side_effects=True, vmem_limit_bytes=VMEM_ALL
         ),
         name="moe",
-    )(partial_sum, hidden, gain, group_t, expert_t, choice_t, w_gate, w_up, w_down)
-
-
-def normed(values, gain):
-    widened = values.astype(jnp.float32)
-    scale = lax.rsqrt(jnp.mean(widened * widened, axis=-1, keepdims=True) + EPSILON)
-    return widened * scale * gain.astype(jnp.float32)
-
-
-def convolve(history, newest, kernel):
-    summed = kernel[-1].astype(jnp.float32) * newest.astype(jnp.float32)
-    for offset in range(history.shape[1]):
-        summed = summed + kernel[offset].astype(jnp.float32) * history[:, offset].astype(
-            jnp.float32
-        )
-    return jax.nn.silu(summed)
-
-
-def project(left, right):
-    return jnp.dot(left, right, preferred_element_type=jnp.float32)
+    )(*operands)
 
 
 def on_device(
@@ -409,66 +591,32 @@
     expert_up,
     expert_down,
 ):
-    tp_count = lax.axis_size("tp")
-    ep_count = lax.axis_size("ep")
-    tp_index = lax.axis_index("tp")
-    seq_rows = hidden.shape[0]
-    mixer_in = normed(hidden, mixer_gain).astype(jnp.bfloat16)
-    gate_new = project(mixer_in, gate_proj).astype(jnp.bfloat16)
-    value_new = project(mixer_in, value_proj).astype(jnp.bfloat16)
-    write_new = project(mixer_in, write_proj).astype(jnp.bfloat16)
-    read_new = project(mixer_in, read_proj).astype(jnp.bfloat16)
-    head_count = step_proj.shape[1] // tp_count
-    head_start = tp_index * head_count
-    step_local = lax.dynamic_slice_in_dim(step_proj, head_start, head_count, 1)
-    bias_local = lax.dynamic_slice_in_dim(step_bias, head_start, head_count, 0)
-    rate_local = jnp.exp(lax.dynamic_slice_in_dim(decay_log, head_start, head_count, 0))
-    skip_local = lax.dynamic_slice_in_dim(skip_gain, head_start, head_count, 0)
-    step_size = jax.nn.softplus(project(mixer_in, step_local) + bias_local)
-    decay = jnp.exp(-step_size * rate_local)
-    value_width = value_proj.shape[1]
-    vector_width = write_proj.shape[1]
-    value_conv = convolve(
-        value_tail,
-        value_new,
-        lax.dynamic_slice_in_dim(value_taps, tp_index * value_width, value_width, 1),
-    )
-    write_conv = convolve(
-        write_tail,
-        write_new,
-        lax.dynamic_slice_in_dim(write_taps, tp_index * vector_width, vector_width, 1),
-    )
-    read_conv = convolve(
-        read_tail,
-        read_new,
-        lax.dynamic_slice_in_dim(read_taps, tp_index * vector_width, vector_width, 1),
-    )
-    state_size = scan_state.shape[3]
-    group_count = vector_width // state_size
-    per_group = head_count // group_count
-    heads_value = value_conv.reshape(seq_rows, head_count, value_width // head_count)
-    heads_write = jnp.repeat(
-        write_conv.reshape(seq_rows, group_count, state_size), per_group, axis=1
-    )
-    heads_read = jnp.repeat(read_conv.reshape(seq_rows, group_count, state_size), per_group, axis=1)
-    new_state = (
-        decay[:, :, None, None] * scan_state
-        + (step_size[:, :, None] * heads_value)[:, :, :, None] * heads_write[:, :, None, :]
-    )
-    mixed_heads = (
-        jnp.einsum("thpn,thn->thp", new_state, heads_read) + skip_local[None, :, None] * heads_value
-    )
-    gated = mixed_heads.reshape(seq_rows, value_width) * jax.nn.silu(gate_new.astype(jnp.float32))
-    grouped = gated.reshape(seq_rows, group_count, value_width // group_count)
-    grouped = grouped * lax.rsqrt(jnp.mean(grouped * grouped, axis=-1, keepdims=True) + EPSILON)
-    gain_local = lax.dynamic_slice_in_dim(group_gain, tp_index * value_width, value_width, 0)
-    mixed = (grouped.reshape(seq_rows, value_width) * gain_local.astype(jnp.float32)).astype(
-        jnp.bfloat16
+    mixer_in, heads, new_state = mix(
+        hidden,
+        mixer_gain,
+        step_proj.T,
+        step_bias.reshape(1, -1),
+        decay_log.reshape(1, -1),
+        skip_gain.reshape(1, -1),
+        value_proj,
+        write_proj,
+        read_proj,
+        value_taps,
+        write_taps,
+        read_taps,
+        value_tail.transpose(1, 0, 2),
+        write_tail.transpose(1, 0, 2),
+        read_tail.transpose(1, 0, 2),
+        scan_state.reshape(SEQ * HIDDEN, 128),
     )
     layer_out = moe(
-        project(mixed, out_proj),
+        mixer_in,
+        gate_proj,
+        heads,
+        group_gain,
+        out_proj,
         hidden,
-        ffn_gain.reshape(1, -1),
+        ffn_gain,
         group_router.T,
         expert_router.T,
         expert_choice.T,
@@ -476,7 +624,7 @@
         expert_up[0],
         expert_down[0],
     )
-    return (layer_out, new_state)
+    return (layer_out, new_state.reshape(scan_state.shape))
 
 
 def solution(mesh):

time: 62.2 us -> 48.3 us (0.78)
  Pallas kernels: 34.2 us -> 46 us
  matrix products: 11.1 us -> 0 us
  other arithmetic: 9.86 us -> 0 us
  local copies, waits for them, and re-layouts: 5.58 us -> 1.42 us
    dot_general x7 -> x0, matrix products: 11.1 us -> none  [the longest x6 6.87 us: project(): return jnp.dot(left, right, preferred_element_type=jnp.float32)]
    pallas_call x0 -> x1, Pallas kernels: none -> 10.7 us  [mix(): pl.pallas_call(mix_kernel, out_shape=(jax.ShapeDtypeStruct((SEQ, WIDTH),...]
    add x2 -> x0, other arithmetic: 6.77 us -> none  [the longest x1 6.69 us: on_device(): decay[:, :, None, None] * scan_state]
    unnamed x39 -> x1, local copies, waits for them, and re-layouts: 4.81 us -> 1.42 us
    mul x3 -> x0, other arithmetic: 1.13 us -> none  [the longest x2 1.03 us: convolve(): summed = kernel[-1].astype(jnp.float32) * newest.astype(jnp.float32)]
    reduce_sum x2 -> x0, other arithmetic: 1.12 us -> none  [the longest x1 1.02 us: normed(): jnp.mean(widened * widened, axis=-1, keepdims=True) + EPSILON]
    pallas_call x1, Pallas kernels: 34.2 us -> 35.3 us  [moe(): pl.pallas_call(moe_kernel, out_shape=jax.ShapeDtypeStruct((SEQ, HALF), BF...]
    convert_element_type x2 -> x0, other arithmetic: 0.83 us -> none  [the longest x1 0.75 us: normed(): return widened * scale * gain.astype(jnp.float32)]
where the time goes in v2:
time: 48.3 us; the launch traced here: 48.1 us
  Pallas kernels  46 us (95%)
  local copies, waits for them, and re-layouts  1.42 us (3%)
  between operations  0.65 us (1%)
    pallas_call x1, Pallas kernels, moe(): pl.pallas_call(moe_kernel, out_shape=jax.ShapeDtypeStruct((SEQ, HALF), BF...  35.3 us
    pallas_call x1, Pallas kernels, mix(): pl.pallas_call(mix_kernel, out_shape=(jax.ShapeDtypeStruct((SEQ, WIDTH),...  10.7 us
    unnamed x1, local copies, waits for them, and re-layouts  1.42 us

profile of v2, /device:TPU:1, one launch (start us, length us, event | category | flops | bytes accessed | tf_op | source)
XLA Modules:
  0.0 48.1 jit_solution(1605215580921355763)
XLA Ops:
  0.6 10.7 %mix.1 = (bf16[22,2048]{1,0:T(8,128)(2,1)}, f32[22,512]{1,0:T(8,128)}, f32[11264,128]{1,0:T(8,128)}) custom-call(bf16[22,2048]{1,0:T(8,128)(2,1)} %refs_5_.1, bf16[2048]{0:T(1024)(128)(2,1)} %refs_1_.2, bf16[16,2048]{1,0:T(8,128)(2,1)} %bitcast.21, f32[1,16]{1,0:T(1,128)} %bitcast.26, f32[1,16]{1,0:T(1,128)} %bitcast.27, f32[1,16]{1,0:T(1,128)} %bitcast.28, ...), custom_call_target="tpu_custom_call" | custom-call | tf_op jit(solution)/shard_map/mix/pallas_call | solution.py:197
  11.4 35.3 %moe.1 = bf16[22,1024]{1,0:T(8,128)(2,1)} custom-call(bf16[22,2048]{1,0:T(8,128)(2,1)} %get-tuple-element.5.refs_0_, bf16[2048,512]{1,0:T(8,128)(2,1)} %refs_1_.3, f32[22,512]{1,0:T(8,128)} %get-tuple-element.6.refs_2_, bf16[1024]{0:T(1024)(128)(2,1)} %refs_3_.1, bf16[512,2048]{1,0:T(8,128)(2,1)} %refs_4_.1, bf16[22,2048]{1,0:T(8,128)(2,1)} %refs_5_.1, ...), custom_call_target="tpu_custom_call" | custom-call | tf_op jit(solution)/shard_map/moe/pallas_call | solution.py:523
  46.7 1.4 %copy.29 = bf16[22,1024]{1,0:T(8,128)(2,1)} copy(bf16[22,1024]{1,0:T(8,128)(2,1)} %moe.1) | data formatting | bytes 90112

commit v3 on v2

--- a/solution.py
+++ b/solution.py
@@ -9,6 +9,8 @@
 EPSILON = 1e-06
 SIDE = 4
 PEERS = 64
+ORDER = (2, 3, 1, 0)
+BATCH = 96
 SLOTS = 3
 WIDTH = 2048
 HALF = 1024
@@ -66,7 +68,7 @@
     tp = lax.axis_index("tp")
 
     def rows_of(c):
-        return pl.ds(pl.multiple_of(c * PAIR, PAIR), PAIR)
+        return pl.ds(c * PAIR, PAIR)
 
     def chunk(c):
         rows = rows_of(c)
@@ -81,8 +83,6 @@
     ]
     for load in loads:
         load.start()
-    for c in range(PAIRS):
-        chunk(c).start()
     for load in loads[:6]:
         load.wait()
 
@@ -111,6 +111,8 @@
             summed = summed + taps[offset : offset + 1, :] * tail_ref[offset].astype(F32)
         return summed * jax.nn.sigmoid(summed)
 
+    for c in range(PAIRS):
+        chunk(c).start()
     for load in loads[6:]:
         load.wait()
     value = convolve(value_tail_ref, project(mixer_in, value_ref[...]), value_taps_ref, HIDDEN)
@@ -148,8 +150,7 @@
     stacked_row = iota((128, 128), 0) % 32
     lane = iota((128, 128), 1)
 
-    @pl.loop(0, PAIRS)
-    def _(c):
+    for c in range(PAIRS):
         chunk(c).wait()
         for g in range(2):
             part = slice(g * 128, (g + 1) * 128)
@@ -164,10 +165,7 @@
             for k in range(2):
                 pieces = []
                 for h in range(4):
-                    rows = pl.ds(
-                        pl.multiple_of(c * PAIR + k * HIDDEN + g * 256 + h * HEAD_DIM, HEAD_DIM),
-                        HEAD_DIM,
-                    )
+                    rows = pl.ds(c * PAIR + k * HIDDEN + g * 256 + h * HEAD_DIM, HEAD_DIM)
                     keep = decays[2 * c + k, g * 4 + h : g * 4 + h + 1, :]
                     new = (
                         keep * state_ref[rows, :]
@@ -241,6 +239,7 @@
         part_ref,
         part_in,
         resid,
+        route,
         send,
         recv,
         recv_sib,
@@ -269,24 +268,37 @@
     ) = refs[27:]
     me = lax.axis_index("ep")
     tp = lax.axis_index("tp")
-    mx, my, mz = me % SIDE, (me // SIDE) % SIDE, me // (SIDE * SIDE)
-
-    def ahead(i):
-        x = (mx + i % SIDE) % SIDE
-        y = (my + (i // SIDE) % SIDE) % SIDE
-        z = (mz + i // (SIDE * SIDE)) % SIDE
-        return (z * SIDE + y) * SIDE + x
-
-    def behind(i):
-        x = (mx + SIDE - i % SIDE) % SIDE
-        y = (my + SIDE - (i // SIDE) % SIDE) % SIDE
-        z = (mz + SIDE - i // (SIDE * SIDE)) % SIDE
-        return (z * SIDE + y) * SIDE + x
+    mx = lax.rem(me, SIDE)
+    my = lax.rem(lax.div(me, SIDE), SIDE)
+    mz = lax.div(me, SIDE * SIDE)
+    xs = [lax.rem(mx + d, SIDE) for d in range(SIDE)]
+    zs = [lax.rem(mz + d, SIDE) * (SIDE * SIDE) for d in range(SIDE)]
+
+    def each_peer(r, sign, act):
+        def line(dy, first):
+            y = lax.rem(my + SIDE + sign * dy, SIDE) * SIDE
+            for dx in range(first, SIDE):
+                act(dy * SIDE + dx, zs[sign * r % SIDE] + y + xs[sign * dx % SIDE])
+
+        if r == 0:
+            line(0, 1)
+
+        @pl.loop(1 if r == 0 else 0, SIDE)
+        def _(dy):
+            line(dy, 0)
 
     sibling = {"tp": 1 - tp}
 
-    def block(i):
-        return pl.ds(pl.multiple_of(i * ROWS, TILES), ROWS)
+    def block(r, j):
+        return pl.ds(pl.multiple_of(r * PLANE + j * ROWS, TILES), ROWS)
+
+    bar = pltpu.get_barrier_semaphore()
+    pl.semaphore_signal(bar, inc=1, device_id=sibling)
+
+    for r in ORDER:
+        each_peer(
+            r, 1, lambda j, peer: pl.semaphore_signal(bar, inc=1, device_id={"ep": peer})
+        )
 
     loads = [
         pltpu.make_async_copy(sources[n], held[n], w_sem.at[n]) for n in range(len(held))
@@ -294,14 +306,31 @@
     for n in [9, 0, 1, 2, 3, 4, 5, 6, 7, 8, 10, 11, 12]:
         loads[n].start()
 
-    bar = pltpu.get_barrier_semaphore()
-    pl.semaphore_signal(bar, inc=1, device_id=sibling)
-
-    @pl.loop(1, PEERS)
-    def _(i):
-        pl.semaphore_signal(bar, inc=1, device_id={"ep": ahead(i)})
-
-    loads[9].wait()
+    for load in loads[:4]:
+        load.wait()
+    gate = project(normed_ref[...], gate_proj[...]).astype(BF).astype(F32)
+    gated = heads_ref[...] * (gate * jax.nn.sigmoid(gate))
+    mixer_cols = pl.ds(pl.multiple_of(tp * HIDDEN, HIDDEN), HIDDEN)
+    group_gain = group_gain_ref[mixer_cols].astype(F32).reshape(1, HIDDEN)
+    mixed = []
+    for g in range(2):
+        cols = slice(g * 256, (g + 1) * 256)
+        part = gated[:, cols]
+        spread_ = lax.rsqrt(jnp.mean(part * part, axis=1, keepdims=True) + EPSILON)
+        mixed.append(part * spread_ * group_gain[:, cols])
+    mixed = jnp.concatenate(mixed, axis=1).astype(BF)
+    loads[4].wait()
+    part_ref[...] = project(mixed, out_proj[...])
+
+    pl.semaphore_wait(bar, PEERS)
+
+    swap = pltpu.make_async_remote_copy(
+        part_ref, part_in, p_send, p_recv, device_id=sibling
+    )
+    swap.start()
+    for load in loads[5:10]:
+        load.wait()
+    resid[16:PAD, :] = jnp.zeros((PAD - 16, WIDTH), F32)
     diagonal = iota((PAD, SEQ), 0) == iota((PAD, SEQ), 1)
     earlier = iota((PAD, SEQ), 1) < iota((PAD, SEQ), 0)
     valid = iota((PAD, 1), 0) < SEQ
@@ -335,31 +364,10 @@
     perm[...] = jnp.where(over_ == (down_ % 16) * TILES + down_ // 16, 1.0, 0.0).astype(BF)
     perm_back[...] = jnp.where(down_ == (over_ % 16) * TILES + over_ // 16, 1.0, 0.0).astype(BF)
 
-    for load in loads[:4]:
-        load.wait()
-    gate = project(normed_ref[...], gate_proj[...]).astype(BF).astype(F32)
-    gated = heads_ref[...] * (gate * jax.nn.sigmoid(gate))
-    mixer_cols = pl.ds(pl.multiple_of(tp * HIDDEN, HIDDEN), HIDDEN)
-    group_gain = group_gain_ref[mixer_cols].astype(F32).reshape(1, HIDDEN)
-    mixed = []
-    for g in range(2):
-        cols = slice(g * 256, (g + 1) * 256)
-        part = gated[:, cols]
-        spread_ = lax.rsqrt(jnp.mean(part * part, axis=1, keepdims=True) + EPSILON)
-        mixed.append(part * spread_ * group_gain[:, cols])
-    mixed = jnp.concatenate(mixed, axis=1).astype(BF)
-    loads[4].wait()
-    part_ref[...] = project(mixed, out_proj[...])
-
-    pl.semaphore_wait(bar, PEERS)
-
-    swap = pltpu.make_async_remote_copy(
-        part_ref, part_in, p_send, p_recv, device_id=sibling
-    )
-    swap.start()
-    for load in loads[5:9]:
-        load.wait()
-    resid[16:PAD, :] = jnp.zeros((PAD - 16, WIDTH), F32)
+    for r in range(SIDE):
+        down = iota((PLANE, SPREAD), 0) + r * PLANE
+        hit = (down == code_rows[0]) | (down == code_rows[1]) | (down == code_rows[2])
+        route[r * PLANE : (r + 1) * PLANE, :] = jnp.where(hit, 1.0, 0.0).astype(BF)
     swap.wait_recv()
     resid[:SEQ, :] = hid_ref[...].astype(F32) + (part_ref[...] + part_in[...])
     total = resid[...]
@@ -379,24 +387,22 @@
         [mine[:, c * 128 : (c + 1) * 128] for c in range(TILES)], axis=0
     ).astype(BF)
 
-    for r in range(SIDE):
-        down = iota((PLANE, SPREAD), 0) + r * PLANE
-        hit = (down == code_rows[0]) | (down == code_rows[1]) | (down == code_rows[2])
-        rows = project(jnp.where(hit, 1.0, 0.0).astype(BF), spread).astype(BF)
+    for r in ORDER:
+        rows = project(route[r * PLANE : (r + 1) * PLANE, :], spread).astype(BF)
         send[r * PLANE : (r + 1) * PLANE, :] = rows
         if r == 0:
             recv[:ROWS, :] = rows[:ROWS, :]
 
-        @pl.loop(1 if r == 0 else 0, 16)
-        def _(j):
-            i = r * 16 + j
+        def dispatch(j, peer, r=r):
             pltpu.make_async_remote_copy(
-                send.at[block(i)],
-                recv.at[block(i)],
+                send.at[block(r, j)],
+                recv.at[block(r, j)],
                 d_send,
                 d_recv.at[r],
-                device_id={"ep": ahead(i)},
+                device_id={"ep": peer},
             ).start()
+
+        each_peer(r, 1, dispatch)
 
     group_exp = jnp.exp(nt_dot(ffn_in, group_ref[...]))
     first = chosen[0].astype(jnp.int32) // GROUP_SIZE
@@ -442,35 +448,40 @@
         part = buffer.at[pl.ds(low, (r + 1) * PLANE - low)]
         return pltpu.make_async_copy(part, part, sem.at[r])
 
-    for r in range(SIDE):
+    own_rows = pl.ds(pl.multiple_of(tp * HALF, HALF), HALF)
+    sib_rows = pl.ds(pl.multiple_of((1 - tp) * HALF, HALF), HALF)
+
+    def arrive(r):
         landed(recv, d_recv, r).wait()
         forward(r).start()
         relay(recv, rows_own, r)
-    for load in loads[10:]:
-        load.wait()
-    for r in range(SIDE):
+
+    def from_sibling(r):
         forward(r).wait_recv()
         relay(recv_sib, rows_sib, r)
 
-    own_rows = pl.ds(pl.multiple_of(tp * HALF, HALF), HALF)
-    sib_rows = pl.ds(pl.multiple_of((1 - tp) * HALF, HALF), HALF)
-    for n in range(2):
-        cols = slice(n * 256, (n + 1) * 256)
-        gated = project(rows_own[...], wg[own_rows, cols]) + project(
-            rows_sib[...], wg[sib_rows, cols]
+    def hand(m):
+        lines_ = pl.ds(m * BATCH, BATCH)
+        return pltpu.make_async_remote_copy(
+            y_out.at[lines_], y_in.at[lines_], s_send.at[m], s_recv.at[m], device_id=sibling
         )
-        upped = project(rows_own[...], wu[own_rows, cols]) + project(
-            rows_sib[...], wu[sib_rows, cols]
-        )
-        act[:, cols] = (gated * jax.nn.sigmoid(gated) * upped).astype(BF)
-
-    y_out[...] = project(act[...], wd[:, sib_rows]).astype(BF)
-    hand = pltpu.make_async_remote_copy(y_out, y_in, s_send, s_recv, device_id=sibling)
-    hand.start()
-    y_own[...] = project(act[...], wd[:, own_rows])
-    hand.wait_recv()
-
-    for r in range(SIDE):
+
+    def expert(m):
+        lines_ = slice(m * BATCH, (m + 1) * BATCH)
+        for n in range(2):
+            cols = slice(n * 256, (n + 1) * 256)
+            gated = project(rows_own[lines_, :], wg[own_rows, cols]) + project(
+                rows_sib[lines_, :], wg[sib_rows, cols]
+            )
+            upped = project(rows_own[lines_, :], wu[own_rows, cols]) + project(
+                rows_sib[lines_, :], wu[sib_rows, cols]
+            )
+            act[lines_, cols] = (gated * jax.nn.sigmoid(gated) * upped).astype(BF)
+        y_out[lines_, :] = project(act[lines_, :], wd[:, sib_rows]).astype(BF)
+        hand(m).start()
+        y_own[lines_, :] = project(act[lines_, :], wd[:, own_rows])
+
+    def give_back(r):
         for b in range(3 * r, 3 * r + 3):
             lines_ = slice(b * 16, (b + 1) * 16)
             summed = (y_own[lines_, :] + y_in[lines_, :].astype(F32)).astype(BF)
@@ -482,19 +493,37 @@
             if b == 0:
                 ret[:ROWS, :] = rows[:ROWS, :]
 
-        @pl.loop(1 if r == 0 else 0, 16)
-        def _(j):
-            i = r * 16 + j
+        def send_back(j, peer):
             pltpu.make_async_remote_copy(
-                back.at[block(i)],
-                ret.at[block(i)],
+                back.at[block(r, j)],
+                ret.at[block(r, j)],
                 r_send,
                 r_recv.at[r],
-                device_id={"ep": behind(i)},
+                device_id={"ep": peer},
             ).start()
 
+        each_peer(r, -1, send_back)
+
+    arrive(2)
+    arrive(3)
+    from_sibling(2)
+    from_sibling(3)
+    for load in loads[10:]:
+        load.wait()
+    expert(1)
+    arrive(1)
+    arrive(0)
+    hand(1).wait_recv()
+    give_back(2)
+    give_back(3)
+    from_sibling(1)
+    from_sibling(0)
+    expert(0)
+    hand(0).wait_recv()
+    give_back(1)
+    give_back(0)
     merged = None
-    for r in range(SIDE):
+    for r in ORDER:
         landed(ret, r_recv, r).wait()
         cols = slice(r * PLANE, (r + 1) * PLANE)
         term = project(comb[:, cols], ret[cols, :])
@@ -506,7 +535,8 @@
         out_ref[:, cols] = line[:SEQ, :].astype(BF)
 
     swap.wait_send()
-    hand.wait_send()
+    for m in range(2):
+        hand(m).wait_send()
     for r in range(SIDE):
         forward(r).wait_send()
     sent = send.at[pl.ds(ROWS, TOTAL - ROWS)]
@@ -530,6 +560,7 @@
             pltpu.VMEM((SEQ, WIDTH), F32),
             pltpu.VMEM((SEQ, WIDTH), F32),
             pltpu.VMEM((PAD, WIDTH), F32),
+            pltpu.VMEM((TOTAL, SPREAD), BF),
             pltpu.VMEM((TOTAL, 128), BF),
             pltpu.VMEM((TOTAL, 128), BF),
             pltpu.VMEM((TOTAL, 128), BF),
@@ -551,8 +582,8 @@
             dma((SIDE,)),
             dma((SIDE,)),
             dma((SIDE,)),
-            dma,
-            dma,
+            dma((2,)),
+            dma((2,)),
             dma,
             dma((SIDE,)),
         ],

time: 48.3 us -> 43.6 us (0.903)
  Pallas kernels: 46 us -> 41.4 us
    pallas_call x1, Pallas kernels: 35.3 us -> 32.2 us  [moe(): pl.pallas_call(moe_kernel, out_shape=jax.ShapeDtypeStruct((SEQ, HALF), BF...]
    pallas_call x1, Pallas kernels: 10.7 us -> 9.19 us  [mix(): pl.pallas_call(mix_kernel, out_shape=(jax.ShapeDtypeStruct((SEQ, WIDTH),...]
where the time goes in v3:
time: 43.6 us; the launch traced here: 43.4 us
  Pallas kernels  41.4 us (95%)
  local copies, waits for them, and re-layouts  1.42 us (3%)
  between operations  0.65 us (1%)
    pallas_call x1, Pallas kernels, moe(): pl.pallas_call(moe_kernel, out_shape=jax.ShapeDtypeStruct((SEQ, HALF), BF...  32.2 us
    pallas_call x1, Pallas kernels, mix(): pl.pallas_call(mix_kernel, out_shape=(jax.ShapeDtypeStruct((SEQ, WIDTH),...  9.19 us
    unnamed x1, local copies, waits for them, and re-layouts  1.42 us

profile of v3, /device:TPU:1, one launch (start us, length us, event | category | flops | bytes accessed | tf_op | source)
XLA Modules:
  0.0 43.4 jit_solution(5110901611737582019)
XLA Ops:
  0.6 9.2 %mix.1 = (bf16[22,2048]{1,0:T(8,128)(2,1)}, f32[22,512]{1,0:T(8,128)}, f32[11264,128]{1,0:T(8,128)}) custom-call(bf16[22,2048]{1,0:T(8,128)(2,1)} %refs_5_.1, bf16[2048]{0:T(1024)(128)(2,1)} %refs_1_.2, bf16[16,2048]{1,0:T(8,128)(2,1)} %bitcast.21, f32[1,16]{1,0:T(1,128)} %bitcast.26, f32[1,16]{1,0:T(1,128)} %bitcast.27, f32[1,16]{1,0:T(1,128)} %bitcast.28, ...), custom_call_target="tpu_custom_call" | custom-call | tf_op jit(solution)/shard_map/mix/pallas_call | solution.py:195
  9.8 32.2 %moe.1 = bf16[22,1024]{1,0:T(8,128)(2,1)} custom-call(bf16[22,2048]{1,0:T(8,128)(2,1)} %get-tuple-element.5.refs_0_, bf16[2048,512]{1,0:T(8,128)(2,1)} %refs_1_.3, f32[22,512]{1,0:T(8,128)} %get-tuple-element.6.refs_2_, bf16[1024]{0:T(1024)(128)(2,1)} %refs_3_.1, bf16[512,2048]{1,0:T(8,128)(2,1)} %refs_4_.1, bf16[22,2048]{1,0:T(8,128)(2,1)} %refs_5_.1, ...), custom_call_target="tpu_custom_call" | custom-call | tf_op jit(solution)/shard_map/moe/pallas_call | solution.py:553
  42.0 1.4 %copy.29 = bf16[22,1024]{1,0:T(8,128)(2,1)} copy(bf16[22,1024]{1,0:T(8,128)(2,1)} %moe.1) | data formatting | bytes 90112

commit v4 on v1

v4 whole, which is shorter than its diff:
```python
import jax
import jax.numpy as jnp
import numpy as np
from jax import lax
from jax.experimental import pallas as pl
from jax.experimental.pallas import tpu as pltpu
from jax.sharding import PartitionSpec as P

GROUP_SIZE = 8
EPSILON = 1e-06
SIDE = 4
PEERS = 64
SLOTS = 3
WIDTH = 2048
HALF = 1024
HIDDEN = 512
TILES = 8
ROWS = SLOTS * TILES
PLANE = 16 * ROWS
TOTAL = PEERS * ROWS
SEQ = 22
PAD = 24
SPREAD = TILES * PAD
HEADS = 8
HEAD_DIM = 64
VECTOR = 256
BF = jnp.bfloat16
F32 = jnp.float32
VMEM_LIMIT = 50 * 1024 * 1024
HOPS = (0, 1, 2, 1)
OFFSETS = sorted(
    ((z, y, x) for z in range(SIDE) for y in range(SIDE) for x in range(SIDE)),
    key=lambda o: (sum(HOPS[d] for d in o), o),
)
RANKS = np.zeros((1, PEERS), np.float32)
for _rank, (_z, _y, _x) in enumerate(OFFSETS):
    RANKS[0, (_z * SIDE + _y) * SIDE + _x] = _rank
PIECES = 4
SPANS = ((0, 4), (4, 10), (10, 16), (16, 22))
SMALL = ("hid", "gain", "step", "bias", "rate", "skip", "choice", "ranks")
TAPS = ("value_taps", "write_taps", "read_taps", "value_tail", "write_tail", "read_tail")
PROJECTIONS = ("value", "write", "read", "gate")
LATER = ("group_gain", "out", "ffn_gain", "group", "expert")
EXPERT = ("wg", "wu", "wd")
INPUTS = SMALL + PROJECTIONS + TAPS + LATER + EXPERT


def nt_dot(left, right):
    return lax.dot_general(left, right, (((1,), (1,)), ((), ())), preferred_element_type=F32)


def project(left, right):
    return jnp.dot(left, right, preferred_element_type=F32)


def iota(shape, dim):
    return lax.broadcasted_iota(jnp.int32, shape, dim)


def silu(x):
    return x * jax.nn.sigmoid(x)


def layer_kernel(*refs):
    count = len(INPUTS)
    sources, state_hbm = refs[:count], refs[count]
    out_ref, state_ref = refs[count + 1 : count + 3]
    held = dict(zip(INPUTS, refs[count + 3 : 2 * count + 3]))
    (
        left,
        left_t,
        right,
        read_t,
        decays,
        acc,
        part_out,
        part_in,
        resid,
        route,
        send,
        recv,
        gate_sum,
        up_sum,
        comb,
        perm,
        perm_back,
        rows_own,
        rows_sib,
        act,
        y_own,
        y_out,
        y_in,
        back,
        ret,
        load_sem,
        state_sem,
        p_send,
        p_recv,
        d_send,
        d_recv,
        f_send,
        f_recv,
        s_send,
        s_recv,
        r_send,
        r_recv,
    ) = refs[2 * count + 3 :]
    me = lax.axis_index("ep")
    tp = lax.axis_index("tp")
    mx = lax.rem(me, SIDE)
    my = lax.rem(lax.div(me, SIDE), SIDE)
    mz = lax.div(me, SIDE * SIDE)
    xs = [lax.rem(mx + d, SIDE) for d in range(SIDE)]
    ys = [lax.rem(my + d, SIDE) * SIDE for d in range(SIDE)]
    zs = [lax.rem(mz + d, SIDE) * (SIDE * SIDE) for d in range(SIDE)]
    sibling = {"tp": 1 - tp}

    def peer(i, sign):
        z, y, x = OFFSETS[i]
        return {"ep": zs[sign * z % SIDE] + ys[sign * y % SIDE] + xs[sign * x % SIDE]}

    loads = {
        name: pltpu.make_async_copy(sources[n], held[name], load_sem.at[n])
        for n, name in enumerate(INPUTS)
    }

    def start(*names):
        for name in names:
            loads[name].start()

    def wait(*names):
        for name in names:
            loads[name].wait()

    start(*SMALL, *TAPS, "value")

    bar = pltpu.get_barrier_semaphore()
    for i in range(PEERS - 1, 0, -1):
        pl.semaphore_signal(bar, inc=1, device_id=peer(i, 1))
    pl.semaphore_signal(bar, inc=1, device_id=sibling)
    start("write", "read")

    def span(n):
        low, high = SPANS[n]
        rows = pl.ds(low * HIDDEN, (high - low) * HIDDEN)
        return pltpu.make_async_copy(state_hbm.at[rows], state_ref.at[rows], state_sem.at[n])

    wait(*SMALL)
    start("gate")
    wide = held["hid"][...].astype(F32)
    scale = lax.rsqrt(jnp.mean(wide * wide, axis=1, keepdims=True) + EPSILON)
    mixer_in = (wide * scale * held["gain"][...].astype(F32).reshape(1, WIDTH)).astype(BF)

    def local_heads(line):
        return jnp.where(tp == 0, line[:, :HEADS], line[:, HEADS:])

    bias = local_heads(held["bias"][...])
    rate = jnp.exp(local_heads(held["rate"][...]))
    skip = local_heads(held["skip"][...])
    raw = local_heads(nt_dot(mixer_in, held["step"][...])) + bias
    step = jnp.maximum(raw, 0.0) + jnp.log1p(jnp.exp(-jnp.abs(raw)))
    decay = jnp.exp(-step * rate)
    for h in range(HEADS):
        decays[:SEQ, h, :] = jnp.broadcast_to(decay[:, h : h + 1], (SEQ, 128))
    span(0).start()
    span(1).start()

    wait("value", *TAPS)

    def convolve(name, newest, width):
        cols = pl.ds(pl.multiple_of(tp * width, width), width)
        taps = held[name + "_taps"][:, cols].astype(F32)
        summed = taps[3:4, :] * newest.astype(BF).astype(F32)
        for offset in range(3):
            summed = summed + taps[offset : offset + 1, :] * held[name + "_tail"][offset].astype(
                F32
            )
        return silu(summed)

    value = convolve("value", project(mixer_in, held["value"][...]), HIDDEN)
    span(2).start()
    span(3).start()
    wait("write", "read")
    start(*LATER)
    write = convolve("write", project(mixer_in, held["write"][...]), VECTOR)
    read = convolve("read", project(mixer_in, held["read"][...]), VECTOR)
    wait("gate")
    gate = silu(project(mixer_in, held["gate"][...]).astype(BF).astype(F32))

    head_of = iota((1, HIDDEN), 1) // HEAD_DIM
    step_wide = jnp.zeros((SEQ, HIDDEN), F32)
    decay_wide = jnp.zeros((SEQ, HIDDEN), F32)
    skip_wide = jnp.zeros((1, HIDDEN), F32)
    for h in range(HEADS):
        step_wide = jnp.where(head_of == h, step[:, h : h + 1], step_wide)
        decay_wide = jnp.where(head_of == h, decay[:, h : h + 1], decay_wide)
        skip_wide = jnp.where(head_of == h, skip[:, h : h + 1], skip_wide)
    drive = step_wide * value
    left[:, :VECTOR] = jnp.zeros((128, VECTOR), F32)
    left[:SEQ, :VECTOR] = read
    for g in range(2):
        part = slice(g * 128, (g + 1) * 128)
        read_t[part, :] = left[:, part].T
    acc[...] = jnp.zeros((HIDDEN, 128), F32)
    lane = iota((128, 128), 1)

    for n, (low, high) in enumerate(SPANS):
        span(n).wait()
        for g in range(2):
            part = slice(g * 128, (g + 1) * 128)
            block_ = slice(g * 256, (g + 1) * 256)
            stream = jnp.concatenate(
                [
                    state_ref[t * HIDDEN + g * 256 : t * HIDDEN + (g + 1) * 256, :].astype(BF)
                    for t in range(low, high)
                ],
                axis=1,
            )
            reader = jnp.concatenate(
                [jnp.where(lane == t, read_t[part, :], 0.0).astype(BF) for t in range(low, high)],
                axis=0,
            )
            acc[block_, :] += project(stream, reader)
    wait("group_gain")
    mixer_cols = pl.ds(pl.multiple_of(tp * HIDDEN, HIDDEN), HIDDEN)
    group_gain = held["group_gain"][mixer_cols].astype(F32).reshape(1, HIDDEN)
    mixed = []
    for g in range(2):
        part = slice(g * 128, (g + 1) * 128)
        cols = slice(g * 256, (g + 1) * 256)
        old = jnp.concatenate(
            [acc[g * 256 + b * 128 : g * 256 + (b + 1) * 128, :].T[:SEQ, :] for b in range(2)],
            axis=1,
        )
        overlap = jnp.sum(write[:, part] * read[:, part], axis=1, keepdims=True)
        heads = (
            decay_wide[:, cols] * old
            + overlap * drive[:, cols]
            + skip_wide[:, cols] * value[:, cols]
        )
        gated = heads * gate[:, cols]
        level = lax.rsqrt(jnp.mean(gated * gated, axis=1, keepdims=True) + EPSILON)
        mixed.append(gated * level * group_gain[:, cols])
    mixed = jnp.concatenate(mixed, axis=1).astype(BF)
    wait("out")
    pl.semaphore_wait(bar, PEERS)

    def swap(n):
        cols = pl.ds(n * HALF, HALF)
        return pltpu.make_async_remote_copy(
            part_out.at[:, cols], part_in.at[:, cols], p_send.at[n], p_recv.at[n], device_id=sibling
        )

    for n in range(2):
        cols = slice(n * HALF, (n + 1) * HALF)
        part_out[:, cols] = project(mixed, held["out"][:, cols])
        swap(n).start()
    start(*EXPERT)
    wait("ffn_gain", "group", "expert")
    resid[16:PAD, :] = jnp.zeros((PAD - 16, WIDTH), F32)
    diagonal = iota((PAD, SEQ), 0) == iota((PAD, SEQ), 1)
    earlier = iota((PAD, SEQ), 1) < iota((PAD, SEQ), 0)
    valid = iota((PAD, 1), 0) < SEQ
    lines = [held["choice"][k : k + 1, :].astype(F32) for k in range(SLOTS)]
    chosen = [jnp.sum(jnp.where(diagonal, line, 0.0), axis=1, keepdims=True) for line in lines]
    codes = []
    for k in range(SLOTS):
        same = jnp.zeros((PAD, SEQ), F32)
        for line in lines:
            same = same + jnp.where((line == chosen[k]) & earlier, 1.0, 0.0)
        rank = jnp.sum(same, axis=1, keepdims=True).astype(jnp.int32)
        number = chosen[k].astype(jnp.int32)
        x = (number % SIDE - mx + SIDE) % SIDE
        y = ((number // SIDE) % SIDE - my + SIDE) % SIDE
        z = (number // (SIDE * SIDE) - mz + SIDE) % SIDE
        seat = jnp.where(iota((PAD, PEERS), 1) == (z * SIDE + y) * SIDE + x, held["ranks"][...], 0.0)
        slot = jnp.sum(seat, axis=1, keepdims=True).astype(jnp.int32) * SLOTS + rank
        codes.append(jnp.where(valid, slot * TILES, -4096))
    lane = iota((PAD, SPREAD), 1)
    on_lane = lane % PAD == iota((PAD, SPREAD), 0)
    tile_of = iota((1, SPREAD), 1) // PAD
    code_rows = [
        jnp.sum(jnp.where(on_lane, code.astype(F32), 0.0), axis=0, keepdims=True).astype(jnp.int32)
        + tile_of
        for code in codes
    ]
    for r in range(SIDE):
        down = iota((PLANE, SPREAD), 0) + r * PLANE
        hit = (down == code_rows[0]) | (down == code_rows[1]) | (down == code_rows[2])
        route[r * PLANE : (r + 1) * PLANE, :] = jnp.where(hit, 1.0, 0.0).astype(BF)
    swap(0).wait_recv()
    swap(1).wait_recv()
    resid[:SEQ, :] = held["hid"][...].astype(F32) + (part_out[...] + part_in[...])
    total = resid[...]
    scale = lax.rsqrt(jnp.mean(total * total, axis=1, keepdims=True) + EPSILON)
    ffn_in = (total * scale * held["ffn_gain"][...].astype(F32).reshape(1, WIDTH)).astype(BF)

    @pl.when(tp == 0)
    def _():
        rows_own[:PAD, :] = ffn_in[:, :HALF]

    @pl.when(tp == 1)
    def _():
        rows_own[:PAD, :] = ffn_in[:, HALF:]

    mine = rows_own[:PAD, :].astype(F32)
    spread = jnp.concatenate(
        [mine[:, c * 128 : (c + 1) * 128] for c in range(TILES)], axis=0
    ).astype(BF)

    def block(i):
        return pl.ds(i * ROWS, ROWS)

    for r in reversed(range(SIDE)):
        rows = project(route[r * PLANE : (r + 1) * PLANE, :], spread).astype(BF)
        send[r * PLANE : (r + 1) * PLANE, :] = rows
        if r == 0:
            recv[:ROWS, :] = rows[:ROWS, :]
        for i in reversed(range(max(16 * r, 1), 16 * r + 16)):
            pltpu.make_async_remote_copy(
                send.at[block(i)], recv.at[block(i)], d_send, d_recv.at[r], device_id=peer(i, 1)
            ).start()

    tile_down = iota((SPREAD, 1), 0) // PAD
    code_cols = [jnp.concatenate([code] * TILES, axis=0) + tile_down for code in codes]

    down_ = iota((128, 128), 0)
    over_ = iota((128, 128), 1)
    perm[...] = jnp.where(over_ == (down_ % 16) * TILES + down_ // 16, 1.0, 0.0).astype(BF)
    perm_back[...] = jnp.where(down_ == (over_ % 16) * TILES + over_ // 16, 1.0, 0.0).astype(BF)
    drive_high = drive.astype(BF).astype(F32)
    write_high = write.astype(BF).astype(F32)
    left[...] = jnp.zeros((128, HIDDEN), F32)
    left[:SEQ, :] = drive_high
    left[32 : 32 + SEQ, :] = drive_high
    left[64 : 64 + SEQ, :] = drive - drive_high
    right[...] = jnp.zeros((128, VECTOR), F32)
    right[:SEQ, :] = write_high
    right[32 : 32 + SEQ, :] = write - write_high
    right[64 : 64 + SEQ, :] = write_high
    for b in range(HIDDEN // 128):
        part = slice(b * 128, (b + 1) * 128)
        left_t[part, :] = left[:, part].T.astype(BF)

    group_exp = jnp.exp(nt_dot(ffn_in, held["group"][...]))
    first = chosen[0].astype(jnp.int32) // GROUP_SIZE
    in_group = iota(group_exp.shape, 1) == first
    chosen_prob = jnp.sum(jnp.where(in_group, group_exp, 0.0), axis=1, keepdims=True) / jnp.sum(
        group_exp, axis=1, keepdims=True
    )
    logits = nt_dot(ffn_in, held["expert"][...])
    place = iota(logits.shape, 1)
    picked = [
        jnp.exp(
            jnp.sum(
                jnp.where(place == number.astype(jnp.int32), logits, 0.0), axis=1, keepdims=True
            )
        )
        for number in chosen
    ]
    below = picked[0] + picked[1] + picked[2]
    gates = [jnp.concatenate([chosen_prob * p / below] * TILES, axis=0) for p in picked]
    for r in range(SIDE):
        over = iota((SPREAD, PLANE), 1) + r * PLANE
        weights = jnp.where(over == code_cols[0], gates[0], 0.0)
        weights = jnp.where(over == code_cols[1], gates[1], weights)
        weights = jnp.where(over == code_cols[2], gates[2], weights)
        comb[:, r * PLANE : (r + 1) * PLANE] = weights.astype(BF)

    def tiles(n):
        return slice(n * 128, (n + 1) * 128)

    def relay(r):
        fresh = jnp.concatenate([recv[tiles(3 * r + k), :] for k in range(3)], axis=1)
        moved = project(perm[...], fresh).astype(BF)
        for k in range(3):
            b = 3 * r + k
            for c in range(TILES):
                rows_own[b * 16 : (b + 1) * 16, tiles(c)] = moved[c * 16 : (c + 1) * 16, tiles(k)]

    def forward(r):
        lines_ = pl.ds(r * 48, 48)
        return pltpu.make_async_remote_copy(
            rows_own.at[lines_], rows_sib.at[lines_], f_send.at[r], f_recv.at[r], device_id=sibling
        )

    def landed(buffer, sem, r):
        low = ROWS if r == 0 else r * PLANE
        part = buffer.at[pl.ds(low, (r + 1) * PLANE - low)]
        return pltpu.make_async_copy(part, part, sem.at[r])

    own_rows = pl.ds(pl.multiple_of(tp * HALF, HALF), HALF)
    sib_rows = pl.ds(pl.multiple_of((1 - tp) * HALF, HALF), HALF)

    def hand(r):
        lines_ = pl.ds(r * 48, 48)
        return pltpu.make_async_remote_copy(
            y_out.at[lines_], y_in.at[lines_], s_send.at[r], s_recv.at[r], device_id=sibling
        )

    def give_back(r):
        stacks = []
        for b in range(3 * r, 3 * r + 3):
            lines_ = slice(b * 16, (b + 1) * 16)
            summed = (y_own[lines_, :] + y_in[lines_, :].astype(F32)).astype(BF)
            stacks.append(jnp.concatenate([summed[:, tiles(c)] for c in range(TILES)], axis=0))
        rows = project(perm_back[...], jnp.concatenate(stacks, axis=1)).astype(BF)
        for k in range(3):
            back[tiles(3 * r + k), :] = rows[:, tiles(k)]
        if r == 0:
            ret[:ROWS, :] = rows[:ROWS, :128]
        for i in reversed(range(max(16 * r, 1), 16 * r + 16)):
            pltpu.make_async_remote_copy(
                back.at[block(i)], ret.at[block(i)], r_send, r_recv.at[r], device_id=peer(i, -1)
            ).start()

    for r in reversed(range(SIDE)):
        landed(recv, d_recv, r).wait()
        relay(r)
        forward(r).start()
    wait(*EXPERT)
    for n in range(2):
        cols = slice(n * 256, (n + 1) * 256)
        gate_sum[:, cols] = project(rows_own[...], held["wg"][own_rows, cols])
        up_sum[:, cols] = project(rows_own[...], held["wu"][own_rows, cols])
    for r in range(SIDE):
        forward(r).wait_recv()
    for n in range(2):
        cols = slice(n * 256, (n + 1) * 256)
        gated = gate_sum[:, cols] + project(rows_sib[...], held["wg"][sib_rows, cols])
        upped = up_sum[:, cols] + project(rows_sib[...], held["wu"][sib_rows, cols])
        act[:, cols] = (silu(gated) * upped).astype(BF)
    y_out[...] = project(act[...], held["wd"][:, sib_rows]).astype(BF)
    for r in reversed(range(SIDE)):
        hand(r).start()
    y_own[...] = project(act[...], held["wd"][:, own_rows])
    for r in reversed(range(SIDE)):
        hand(r).wait_recv()
        give_back(r)
    stacked_row = iota((128, 128), 0) % 32
    for c in range(SEQ // 2):
        pair = [2 * c, 2 * c + 1]
        for g in range(2):
            part = slice(g * 128, (g + 1) * 128)
            outer = project(
                left_t[g * 256 : (g + 1) * 256, :],
                jnp.concatenate(
                    [jnp.where(stacked_row == t, right[:, part], 0.0) for t in pair], axis=1
                ).astype(BF),
            )
            for k, t in enumerate(pair):
                for h in range(4):
                    rows = pl.ds(t * HIDDEN + g * 256 + h * HEAD_DIM, HEAD_DIM)
                    keep = decays[t, g * 4 + h : g * 4 + h + 1, :]
                    state_ref[rows, :] = (
                        keep * state_ref[rows, :]
                        + outer[h * HEAD_DIM : (h + 1) * HEAD_DIM, k * 128 : (k + 1) * 128]
                    )
    merged = None
    for r in range(SIDE):
        landed(ret, r_recv, r).wait()
        cols = slice(r * PLANE, (r + 1) * PLANE)
        term = project(comb[:, cols], ret[cols, :])
        merged = term if merged is None else merged + term
    half = resid[:, own_rows]
    for c in range(TILES):
        cols = slice(c * 128, (c + 1) * 128)
        line = half[:, cols] + merged[c * PAD : (c + 1) * PAD, :]
        out_ref[:, cols] = line[:SEQ, :].astype(BF)

    for n in range(2):
        swap(n).wait_send()
    for r in range(SIDE):
        hand(r).wait_send()
    for r in range(SIDE):
        forward(r).wait_send()
    sent = send.at[pl.ds(ROWS, TOTAL - ROWS)]
    pltpu.make_async_copy(sent, sent, d_send).wait()
    gone = back.at[pl.ds(ROWS, TOTAL - ROWS)]
    pltpu.make_async_copy(gone, gone, r_send).wait()


def layer(*operands):
    dma = pltpu.SemaphoreType.DMA
    slots = PEERS * SLOTS
    pinned = [pltpu.with_memory_space_constraint(x, pltpu.HBM) for x in operands]
    return pl.pallas_call(
        layer_kernel,
        out_shape=(pltpu.VMEM((SEQ, HALF), BF), pltpu.VMEM((SEQ * HIDDEN, 128), F32)),
        in_specs=[pl.BlockSpec(memory_space=pltpu.HBM)] * len(operands),
        out_specs=(pl.BlockSpec(memory_space=pltpu.VMEM),) * 2,
        scratch_shapes=[pltpu.VMEM(x.shape, x.dtype) for x in operands[:-1]]
        + [
            pltpu.VMEM((128, HIDDEN), F32),
            pltpu.VMEM((HIDDEN, 128), BF),
            pltpu.VMEM((128, VECTOR), F32),
            pltpu.VMEM((VECTOR, 128), F32),
            pltpu.VMEM((PAD, HEADS, 128), F32),
            pltpu.VMEM((HIDDEN, 128), F32),
            pltpu.VMEM((SEQ, WIDTH), F32),
            pltpu.VMEM((SEQ, WIDTH), F32),
            pltpu.VMEM((PAD, WIDTH), F32),
            pltpu.VMEM((TOTAL, SPREAD), BF),
            pltpu.VMEM((TOTAL, 128), BF),
            pltpu.VMEM((TOTAL, 128), BF),
            pltpu.VMEM((slots, HIDDEN), F32),
            pltpu.VMEM((slots, HIDDEN), F32),
            pltpu.VMEM((SPREAD, TOTAL), BF),
            pltpu.VMEM((128, 128), BF),
            pltpu.VMEM((128, 128), BF),
            pltpu.VMEM((slots, HALF), BF),
            pltpu.VMEM((slots, HALF), BF),
            pltpu.VMEM((slots, HIDDEN), BF),
            pltpu.VMEM((slots, HALF), F32),
            pltpu.VMEM((slots, HALF), BF),
            pltpu.VMEM((slots, HALF), BF),
            pltpu.VMEM((TOTAL, 128), BF),
            pltpu.VMEM((TOTAL, 128), BF),
            dma((len(INPUTS),)),
            dma((len(SPANS),)),
            dma((2,)),
            dma((2,)),
            dma,
            dma((SIDE,)),
            dma((SIDE,)),
            dma((SIDE,)),
            dma((SIDE,)),
            dma((SIDE,)),
            dma,
            dma((SIDE,)),
        ],
        compiler_params=pltpu.CompilerParams(
            collective_id=0, has_side_effects=True, vmem_limit_bytes=VMEM_LIMIT
        ),
        name="layer",
    )(*pinned)


def finish_kernel(rows_ref, state_ref, rows_out, state_out, sems):
    span = SEQ * HIDDEN // PIECES
    copies = [
        pltpu.make_async_copy(
            state_ref.at[pl.ds(n * span, span)], state_out.at[pl.ds(n * span, span)], sems.at[n]
        )
        for n in range(PIECES)
    ]
    copies.append(pltpu.make_async_copy(rows_ref, rows_out, sems.at[PIECES]))
    for copy in copies:
        copy.start()
    for copy in copies:
        copy.wait()


def finish(rows, state):
    hbm = pl.BlockSpec(memory_space=pltpu.HBM)
    vmem = pl.BlockSpec(memory_space=pltpu.VMEM)
    return pl.pallas_call(
        finish_kernel,
        out_shape=(
            jax.ShapeDtypeStruct(rows.shape, rows.dtype),
            jax.ShapeDtypeStruct(state.shape, state.dtype),
        ),
        in_specs=[vmem, vmem],
        out_specs=(hbm, hbm),
        scratch_shapes=[pltpu.SemaphoreType.DMA((PIECES + 1,))],
        compiler_params=pltpu.CompilerParams(vmem_limit_bytes=1024 * 1024),
        name="finish",
    )(*[pltpu.with_memory_space_constraint(x, pltpu.VMEM) for x in (rows, state)])


def on_device(
    hidden,
    mixer_gain,
    gate_proj,
    value_proj,
    write_proj,
    read_proj,
    step_proj,
    step_bias,
    decay_log,
    skip_gain,
    value_taps,
    write_taps,
    read_taps,
    value_tail,
    write_tail,
    read_tail,
    scan_state,
    group_gain,
    out_proj,
    ffn_gain,
    group_router,
    expert_router,
    expert_choice,
    expert_gate,
    expert_up,
    expert_down,
):
    layer_out, new_state = finish(*layer(
        hidden,
        mixer_gain,
        step_proj.T,
        step_bias.reshape(1, -1),
        decay_log.reshape(1, -1),
        skip_gain.reshape(1, -1),
        expert_choice.T,
        jnp.asarray(RANKS),
        value_proj,
        write_proj,
        read_proj,
        gate_proj,
        value_taps,
        write_taps,
        read_taps,
        value_tail.transpose(1, 0, 2),
        write_tail.transpose(1, 0, 2),
        read_tail.transpose(1, 0, 2),
        group_gain,
        out_proj,
        ffn_gain,
        group_router.T,
        expert_router.T,
        expert_gate[0],
        expert_up[0],
        expert_down[0],
        scan_state.reshape(SEQ * HIDDEN, 128),
    ))
    return (layer_out, new_state.reshape(scan_state.shape))


def solution(mesh):
    placed = (
        P("ep", None),
        P(),
        P(None, "tp"),
        P(None, "tp"),
        P(None, "tp"),
        P(None, "tp"),
        P(),
        P(),
        P(),
        P(),
        P(),
        P(),
        P(),
        P("ep", None, "tp"),
        P("ep", None, "tp"),
        P("ep", None, "tp"),
        P("ep", "tp", None, None),
        P(),
        P("tp", None),
        P(),
        P(),
        P(),
        P("ep", None),
        P("ep", None, "tp"),
        P("ep", None, "tp"),
        P("ep", "tp", None),
    )
    return jax.shard_map(
        on_device,
        mesh=mesh,
        in_specs=placed,
        out_specs=(P("ep", "tp"), P("ep", "tp", None, None)),
        check_vma=False,
    )
```

time: 62.2 us -> 36 us (0.58)
  matrix products: 11.1 us -> 0 us
  other arithmetic: 9.86 us -> 0 us
  local copies, waits for them, and re-layouts: 5.58 us -> 0 us
  Pallas kernels: 34.2 us -> 35.2 us
    dot_general x7 -> x0, matrix products: 11.1 us -> none  [the longest x6 6.87 us: project(): return jnp.dot(left, right, preferred_element_type=jnp.float32)]
    add x2 -> x0, other arithmetic: 6.77 us -> none  [the longest x1 6.69 us: on_device(): decay[:, :, None, None] * scan_state]
    unnamed x39 -> x0, local copies, waits for them, and re-layouts: 4.81 us -> none
    mul x3 -> x0, other arithmetic: 1.13 us -> none  [the longest x2 1.03 us: convolve(): summed = kernel[-1].astype(jnp.float32) * newest.astype(jnp.float32)]
    reduce_sum x2 -> x0, other arithmetic: 1.12 us -> none  [the longest x1 1.02 us: normed(): jnp.mean(widened * widened, axis=-1, keepdims=True) + EPSILON]
    pallas_call x1 -> x2, Pallas kernels: 34.2 us -> 35.2 us  [the longest x1 32.6 us: layer(): pl.pallas_call(layer_kernel, out_shape=(pltpu.VMEM((SEQ, HALF), BF), pltp...]
    convert_element_type x2 -> x0, other arithmetic: 0.83 us -> none  [the longest x1 0.75 us: normed(): return widened * scale * gain.astype(jnp.float32)]
where the time goes in v4:
time: 36 us; the launch traced here: 35.8 us
  Pallas kernels  35.2 us (98%)
  between operations  0.65 us (2%)
    pallas_call x1, Pallas kernels, layer(): pl.pallas_call(layer_kernel, out_shape=(pltpu.VMEM((SEQ, HALF), BF), pltp...  32.6 us
    pallas_call x1, Pallas kernels, finish(): pl.pallas_call(finish_kernel, out_shape=(jax.ShapeDtypeStruct(rows.shape,...  2.57 us

profile of v4, /device:TPU:1, one launch (start us, length us, event | category | flops | bytes accessed | tf_op | source)
XLA Modules:
  0.0 35.8 jit_solution(12758762405761407188)
XLA Ops:
  0.6 32.6 %layer.1 = (bf16[22,1024]{1,0:T(8,128)(2,1)S(1)}, f32[11264,128]{1,0:T(8,128)S(1)}) custom-call(bf16[22,2048]{1,0:T(8,128)(2,1)} %refs_0_.1, bf16[2048]{0:T(1024)(128)(2,1)} %refs_1_.1, bf16[16,2048]{1,0:T(8,128)(2,1)} %bitcast.21, f32[1,16]{1,0:T(1,128)} %bitcast.26, f32[1,16]{1,0:T(1,128)} %bitcast.27, f32[1,16]{1,0:T(1,128)} %bitcast.28, ...), custom_call_target="tpu_custom_call" | custom-call | tf_op jit(solution)/shard_map/layer/pallas_call | solution.py:487
  33.3 2.6 %finish.1 = (bf16[22,1024]{1,0:T(8,128)(2,1)}, f32[11264,128]{1,0:T(8,128)}) custom-call(bf16[22,1024]{1,0:T(8,128)(2,1)S(1)} %get-tuple-element.6.rows_ref, f32[11264,128]{1,0:T(8,128)S(1)} %get-tuple-element.7.state_ref), custom_call_target="tpu_custom_call" | custom-call | tf_op jit(solution)/shard_map/finish/pallas_call | solution.py:557
